TPU v7x, 256 devices: a whole 4x4x8 slice. The times are simulated.
256 devices in a mesh: ep: 16 (over y, x), tp: 16 (over z, core).
Axes of the slice: x: 4, y: 4, z: 8, core: 2. Of those that a mesh axis runs over, the one named last changes fastest.
Arguments:
- tokens: bfloat16 [1024, 2048], P('ep', 'tp'), may hold values from -64 to 64
- mixer_gain: float32 [2048], replicated, may hold values from 0.1 to 1.9
- expert_gain: float32 [2048], replicated, may hold values from 0.1 to 1.9
- query_weight: bfloat16 [2048, 1024], P(None, 'tp'), may hold values from -0.125 to 0.125
- key_weight: bfloat16 [2048, 1024], P(None, 'tp'), may hold values from -0.125 to 0.125
- value_weight: bfloat16 [2048, 4, 256], P(None, None, 'tp'), may hold values from -0.125 to 0.125
- outgate_weight: bfloat16 [2048, 4, 256], P(None, None, 'tp'), may hold values from -0.125 to 0.125
- ingate_weight: bfloat16 [2048, 4], replicated, may hold values from -0.125 to 0.125
- forget_weight: bfloat16 [2048, 4], replicated, may hold values from -0.125 to 0.125
- forget_bias: float32 [4], replicated, may hold values from -1 to 4
- mixout_weight: bfloat16 [1024, 2048], replicated, may hold values from -0.1875 to 0.1875
- memory_state: float32 [1024, 4, 256, 256], P('ep', None, 'tp'), may hold values from -0.6 to 0.6
- norm_state: float32 [1024, 4, 256], P('ep'), may hold values from -0.6 to 0.6
- max_state: float32 [1024, 4], P('ep'), may hold values from -4 to 4
- expert_gate: bfloat16 [256, 2048, 256], P(('ep', 'tp')), may hold values from -0.125 to 0.125
- expert_up: bfloat16 [256, 2048, 256], P(('ep', 'tp')), may hold values from -0.125 to 0.125
- expert_down: bfloat16 [256, 256, 2048], P(('ep', 'tp')), may hold values from -0.1875 to 0.1875
- routes: int32 [1024, 2], P('ep'), may hold values from 0 to 63, all different within a row; in each aligned block of 64 rows (0 to 63, 64 to 127, ...) at most 4 rows name the same one
- route_weights: float32 [1024, 2], P('ep'), may hold values from 0.1 to 1
Outputs:
- mixed_out: bfloat16 [1024, 2048], P('ep', 'tp')
- memory_next: float32 [1024, 4, 256, 256], P('ep', None, 'tp')
- norm_next: float32 [1024, 4, 256], P('ep')
- max_next: float32 [1024, 4], P('ep')
Inputs may be any that keep to these rules, and one draw needn't show every extreme that they name: `routes`: each row names 2 different experts; in the rows of one index of ep (aligned blocks of 64 rows) no expert is named by more than 4 rows, a bound that some block reaches.
All inputs are finite; a program needn't handle non-finite values.
Results may differ from a plain program's by a relative error of at most 0.0079.
Values may be sent and summed in bfloat16 or wider, within the bound.
A program may use at most 64 MiB of HBM per device.

v0:
```python
import jax
import jax.numpy as jnp
from jax import lax
from jax.sharding import PartitionSpec as P

FF_SPLIT = 4


eps = 1e-06


def gather_turned(arrays, axis, dims):
    turned = [jnp.moveaxis(a, dim, 0) for a, dim in zip(arrays, dims)]
    both = jnp.concatenate([t.reshape(len(t), -1) for t in turned], axis=1)
    result, at, gathered = (lax.all_gather(both, axis, axis=0, tiled=True), 0, [])
    for t, dim in zip(turned, dims):
        share = result[:, at : at + t[0].size].reshape(-1, *t.shape[1:])
        gathered.append(jnp.moveaxis(share, 0, dim))
        at += t[0].size
    return tuple(gathered)


def in_order(pieces, dim):
    shape = list(pieces.shape[1:])
    shape[dim] *= pieces.shape[0]
    return jnp.moveaxis(pieces, 0, dim).reshape(shape)


def from_everyone(shard, axis):
    copies = jnp.broadcast_to(shard, (lax.axis_size(axis), *shard.shape))
    return lax.all_to_all(copies, axis, split_axis=0, concat_axis=0, tiled=True)


def gathered_copies(shard, axis, dim):
    return in_order(from_everyone(shard, axis), dim)


def cut_along(shard, dim, devices):
    before, after = (shard.shape[:dim], shard.shape[dim + 1 :])
    return jnp.moveaxis(shard.reshape(*before, devices, -1, *after), dim, 0)


def sent_and_summed(shard, axis, dim):
    devices = lax.axis_size(axis)
    pieces = lax.all_to_all(cut_along(shard, dim, devices), axis, 0, 0, tiled=True)
    return jnp.sum(pieces.astype(jnp.float32), axis=0)


def rms_inverse(row_float):
    return lax.rsqrt(jnp.mean(row_float * row_float, axis=1, keepdims=True) + eps)


def slot_targets(routes, expert_count, capacity):
    flat_routes = routes.reshape(-1)
    onehot = (flat_routes[:, None] == jnp.arange(expert_count, dtype=jnp.int32)[None, :]).astype(
        jnp.int32
    )
    counts = jnp.cumsum(onehot, axis=0)
    slot_rank = jnp.sum(onehot * (counts - 1), axis=1)
    return flat_routes * capacity + slot_rank


def local(
    tokens,
    mixer_gain,
    expert_gain,
    query_weight,
    key_weight,
    value_weight,
    outgate_weight,
    ingate_weight,
    forget_weight,
    forget_bias,
    mixout_weight,
    memory_state,
    norm_state,
    max_state,
    expert_gate,
    expert_up,
    expert_down,
    routes,
    route_weights,
):
    seq_count, own_width = tokens.shape
    model_width = mixer_gain.shape[0]
    head_count = ingate_weight.shape[1]
    head_dim = norm_state.shape[2]
    local_values = value_weight.shape[2]
    offset = lax.axis_index("tp") * own_width
    full_rows = lax.all_gather(tokens, "tp", axis=1, tiled=True)
    full_float = full_rows.astype(jnp.float32)
    inverse = rms_inverse(full_float)
    scaled = (full_float * mixer_gain).astype(jnp.bfloat16)
    query_own = inverse * jnp.dot(scaled, query_weight, preferred_element_type=jnp.float32)
    key_own = (
        inverse
        * jnp.dot(scaled, key_weight, preferred_element_type=jnp.float32)
        * head_dim ** (-0.5)
    )
    query_cols, key_cols = gather_turned((query_own, key_own), "tp", (1, 1))
    query_full = query_cols.reshape(seq_count, head_count, head_dim)
    key_full = key_cols.reshape(seq_count, head_count, head_dim)
    values = (
        inverse
        * jnp.dot(
            scaled,
            value_weight.reshape(model_width, head_count * local_values),
            preferred_element_type=jnp.float32,
        )
    ).reshape(seq_count, head_count, local_values)
    outgate = (
        inverse
        * jnp.dot(
            scaled,
            outgate_weight.reshape(model_width, head_count * local_values),
            preferred_element_type=jnp.float32,
        )
    ).reshape(seq_count, head_count, local_values)
    ingate = inverse * jnp.dot(scaled, ingate_weight, preferred_element_type=jnp.float32)
    logforget = jax.nn.log_sigmoid(
        inverse * jnp.dot(scaled, forget_weight, preferred_element_type=jnp.float32) + forget_bias
    )
    max_next = jnp.maximum(logforget + max_state, ingate)
    decay_rate = jnp.exp(logforget + max_state - max_next)
    inflow = jnp.exp(ingate - max_next)
    memory_next = (
        decay_rate[:, :, None, None] * memory_state
        + inflow[:, :, None, None] * values[:, :, :, None] * key_full[:, :, None, :]
    )
    norm_next = decay_rate[:, :, None] * norm_state + inflow[:, :, None] * key_full
    numerator = jnp.einsum(
        "shvk,shk->shv", memory_next, query_full, precision=lax.Precision.HIGHEST
    )
    denominator = jnp.maximum(jnp.abs(jnp.sum(norm_next * query_full, axis=2)), jnp.exp(-max_next))
    gated_heads = (jax.nn.sigmoid(outgate) * (numerator / denominator[:, :, None])).astype(
        jnp.bfloat16
    )
    heads_full = gathered_copies(gated_heads, "tp", 2).reshape(seq_count, head_count * head_dim)
    group_count = lax.axis_size("ep")
    width_count = lax.axis_size("tp")
    block_count = expert_gate.shape[0]
    local_experts = block_count * width_count // FF_SPLIT
    expert_count = local_experts * group_count
    topk_count = routes.shape[1]
    capacity = max(2, 2 * seq_count * topk_count // expert_count)
    slot_count = expert_count * capacity
    targets = slot_targets(routes, expert_count, capacity)
    slot_iota = jnp.arange(slot_count, dtype=jnp.int32)
    picker = (
        (targets[:, None] == slot_iota[None, :])
        .astype(jnp.bfloat16)
        .reshape(seq_count, topk_count, slot_count)
        .sum(axis=1)
    )
    middle_full = (
        full_float + jnp.dot(heads_full, mixout_weight, preferred_element_type=jnp.float32)
    ).astype(jnp.bfloat16)
    middle_own = lax.dynamic_slice_in_dim(middle_full, offset, own_width, 1)
    middle_float = middle_full.astype(jnp.float32)
    normed_full = (middle_float * rms_inverse(middle_float) * expert_gain).astype(jnp.bfloat16)
    buffer = jnp.einsum(
        "sr,sd->rd", picker, normed_full, preferred_element_type=jnp.float32
    ).astype(jnp.bfloat16)
    expert_rows = lax.all_to_all(
        buffer.reshape(group_count, local_experts * capacity, normed_full.shape[1]),
        "ep",
        split_axis=0,
        concat_axis=0,
        tiled=True,
    )
    row_block = expert_rows.reshape(group_count, local_experts, capacity, model_width)
    block_expert = (
        lax.axis_index("tp") * block_count + jnp.arange(block_count, dtype=jnp.int32)
    ) // FF_SPLIT
    block_rows = jnp.take(row_block, block_expert, axis=1)
    gate_part = jnp.einsum(
        "glcd,ldf->glcf", block_rows, expert_gate, preferred_element_type=jnp.float32
    )
    up_part = jnp.einsum(
        "glcd,ldf->glcf", block_rows, expert_up, preferred_element_type=jnp.float32
    )
    hidden = (jax.nn.silu(gate_part) * up_part).astype(jnp.bfloat16)
    down_part = jnp.einsum(
        "glcf,lfd->glcd", hidden, expert_down, preferred_element_type=jnp.float32
    )
    owner = (block_expert[:, None] == jnp.arange(local_experts, dtype=jnp.int32)[None, :]).astype(
        jnp.float32
    )
    term = jnp.einsum("glcd,le->gecd", down_part, owner, precision=lax.Precision.HIGHEST).reshape(
        group_count, local_experts * capacity, model_width
    )
    down_share = sent_and_summed(term.astype(jnp.bfloat16), "tp", 2)
    outgoing = down_share.astype(jnp.bfloat16)
    returned = lax.all_to_all(outgoing, "ep", split_axis=0, concat_axis=0, tiled=True).reshape(
        slot_count, own_width
    )
    shares = route_weights / jnp.sum(route_weights, axis=1, keepdims=True)
    matches = (
        targets.reshape(seq_count, topk_count)[:, :, None] == slot_iota[None, None, :]
    ).astype(jnp.float32)
    combiner = jnp.sum(matches * shares[:, :, None], axis=1)
    expert_sum = jnp.dot(combiner, returned.astype(jnp.float32), precision=lax.Precision.HIGHEST)
    mixed_out = (middle_own.astype(jnp.float32) + expert_sum).astype(jnp.bfloat16)
    return (mixed_out, memory_next, norm_next, max_next)


def solution(mesh):
    in_specs = (
        P("ep", "tp"),
        P(),
        P(),
        P(None, "tp"),
        P(None, "tp"),
        P(None, None, "tp"),
        P(None, None, "tp"),
        P(),
        P(),
        P(),
        P(),
        P("ep", None, "tp", None),
        P("ep", None, None),
        P("ep", None),
        P(("ep", "tp"), None, None),
        P(("ep", "tp"), None, None),
        P(("ep", "tp"), None, None),
        P("ep", None),
        P("ep", None),
    )
    out_specs = (P("ep", "tp"), P("ep", None, "tp", None), P("ep", None, None), P("ep", None))
    return jax.shard_map(local, mesh=mesh, in_specs=in_specs, out_specs=out_specs, check_vma=False)
```

profile of v0, /device:TPU:1, one launch (start us, length us, event | category | flops | bytes accessed | tf_op | source)
XLA Modules:
  0.0 145.8 jit_solution(12836255112575005096)
XLA Ops:
  0.6 0.0 copy-start
  0.6 0.0 copy-start.7
  0.7 0.0 copy-start.1
  0.7 22.4 %all_gather.6 = bf16[64,2048]{1,0:T(8,128)(2,1)S(1)} all-gather(bf16[64,128]{1,0:T(8,128)(2,1)} %param.19), channel_id=1, replica_groups=mesh['ep'=16,'tp'=16] {'tp'}, dimensions={1}, use_global_device_ids=true | all-gather | bytes 278528 | tf_op jit(solution)/shard_map/all_gather | solution.py:90
  23.1 0.2 fusion.23
  23.2 0.9 convolution_multiply_fusion.4
  24.1 0.9 subtract_exponential_fusion.1
  25.1 0.0 copy-start.3
  25.1 0.1 copy.145
  25.2 0.1 copy.137
  25.3 1.2 fusion.5
  26.5 1.2 fusion.6
  27.7 0.1 copy.142
  27.8 15.9 %all_gather.7 = f32[1024,128]{1,0:T(8,128)S(1)} all-gather(f32[64,128]{1,0:T(8,128)S(1)} %copy.142), channel_id=1, replica_groups=mesh['ep'=16,'tp'=16] {'tp'}, dimensions={0}, use_global_device_ids=true | all-gather | bytes 557056 | tf_op jit(solution)/shard_map/all_gather | solution.py:15
  43.7 0.2 fusion.60
  43.9 0.2 copy.143
  44.1 0.2 copy.165
  44.3 0.0 copy-done.1
  44.3 0.9 multiply_reduce_fusion.1
  45.2 0.1 copy.148
  45.3 0.0 copy-done.7
  45.3 1.2 convolution_multiply_fusion.2
  46.5 0.1 copy.138
  46.6 0.1 copy.139
  46.7 0.0 copy-start.6
  46.7 0.0 copy-start.4
  46.7 4.5 %multiply_reduce_fusion = (f32[64,4,16]{2,1,0:T(4,128)S(1)}, f32[64,4,16,256]{3,2,1,0:T(8,128)}) fusion(f32[64,4,256]{2,1,0:T(4,128)S(1)} %copy.165, f32[64,4,256]{2,1,0:T(4,128)S(1)} %copy.143, f32[64,4,16]{2,1,0:T(4,128)S(1)} %copy.139, f32[64,4,16,256]{3,2,1,0:T(8,128)} %param.30, f32[64,4]{1,0:T(8,128)S(1)} %copy.137), kind=kLoop, calls=%fused_computation | loop fusion | flops 5238784 | bytes 8946688
  51.2 0.0 copy-done.3
  51.2 0.1 copy.163
  51.3 0.2 fusion.10
  51.6 0.1 copy.136
  51.7 0.9 reshape.211
  52.6 4.4 %all-to-all-start = ((bf16[16,2,2048]{2,1,0:T(2,128)(2,1)}), bf16[16,2,2048]{2,1,0:T(2,128)(2,1)S(1)}, u32[]{:S(2)}, u32[]{:S(2)}) async-start(bf16[16,2,2048]{2,1,0:T(2,128)(2,1)} %reshape.211), calls=%async_computation | async-start | bytes 262144 | tf_op jit(solution)/shard_map/all_to_all | solution.py:31
  57.0 0.1 copy.150
  57.1 0.1 eq.53
  57.3 0.1 fusion.47
  57.4 0.2 reduce_window_sum.11
  57.5 0.2 select_reduce_fusion.1
  57.7 0.1 reduce_sum.83
  57.9 0.1 copy.151
  57.9 0.1 fusion.41
  58.1 7.9 %all-to-all-done = bf16[16,2,2048]{2,1,0:T(2,128)(2,1)S(1)} async-done(((bf16[16,2,2048]{2,1,0:T(2,128)(2,1)}), bf16[16,2,2048]{2,1,0:T(2,128)(2,1)S(1)}, u32[]{:S(2)}, u32[]{:S(2)}) %all-to-all-start) | async-done | bytes 131104 | tf_op jit(solution)/shard_map/all_to_all | solution.py:31
  65.9 0.2 reshape.212
  66.2 3.2 %fusion.20 = (f32[64]{0:T(128)S(1)}, bf16[64,2048]{1,0:T(8,128)(2,1)S(1)}) fusion(bf16[64,1024]{0,1:T(8,128)(2,1)S(1)} %bitcast.101, bf16[1024,2048]{1,0:T(8,128)(2,1)} %param.29, bf16[64,2048]{1,0:T(8,128)(2,1)S(1)} %all_gather.6), kind=kOutput, calls=%fused_computation.36 | convolution fusion | flops 269221824 | bytes 4849920 | tf_op jit(solution)/shard_map/dot_general | solution.py:156
  69.4 0.0 copy-done.2
  69.4 1.5 %convolution_convert_fusion = bf16[256,2048]{1,0:T(8,128)(2,1)} fusion(bf16[64,256]{1,0:T(8,128)(2,1)S(1)} %fusion.41, bf16[64,2048]{1,0:T(8,128)(2,1)S(1)} %get-tuple-element.24, f32[2048]{0:T(1024)S(1)} %copy-done.2, f32[64]{0:T(128)S(1)} %add_rsqrt_fusion), kind=kOutput, calls=%fused_computation.2 | convolution fusion | flops 68157440 | bytes 1351936 | tf_op jit(solution)/shard_map/sr,sd->rd/dot_general | solution.py:161
  70.9 6.8 %all-to-all-start.1 = ((bf16[16,16,2048]{2,1,0:T(8,128)(2,1)}), bf16[16,16,2048]{2,1,0:T(8,128)(2,1)S(1)}, u32[]{:S(2)}, u32[]{:S(2)}) async-start(bf16[16,16,2048]{2,1,0:T(8,128)(2,1)} %bitcast.18), calls=%async_computation.1 | async-start | bytes 2097152 | tf_op jit(solution)/shard_map/all_to_all | solution.py:164
  77.7 18.2 %all-to-all-done.1 = bf16[16,16,2048]{2,1,0:T(8,128)(2,1)S(1)} async-done(((bf16[16,16,2048]{2,1,0:T(8,128)(2,1)}), bf16[16,16,2048]{2,1,0:T(8,128)(2,1)S(1)}, u32[]{:S(2)}, u32[]{:S(2)}) %all-to-all-start.1) | async-done | bytes 1048608 | tf_op jit(solution)/shard_map/all_to_all | solution.py:164
  95.9 0.6 copy.152
  96.5 1.5 %convolution_bitcast_fusion.1 = f32[16,1,4,256]{3,0,2,1:T(8,128)S(1)} fusion(bf16[1,2048,256]{2,1,0:T(8,128)(2,1)} %param.33, bf16[16,4,4,2048]{3,0,2,1:T(8,128)(2,1)S(1)} %bitcast.97, s32[]{:T(128)} %bitcast.20, pred[]{:T(512)} %bitcast.17), kind=kOutput, calls=%fused_computation.7 | convolution fusion | flops 67239936 | bytes 1376261 | tf_op jit(solution)/shard_map/glcd,ldf->glcf/dot_general | solution.py:176
  98.0 0.0 copy-done
  98.0 2.0 %fusion.14 = f32[16,4,2048]{2,0,1:T(8,128)S(1)} fusion(bf16[1,256,2048]{2,1,0:T(8,128)(2,1)S(1)} %copy-done, bf16[1,2048,256]{2,1,0:T(8,128)(2,1)} %param.34, bf16[16,4,4,2048]{3,0,2,1:T(8,128)(2,1)S(1)} %bitcast.98, s32[]{:T(128)} %bitcast.20, pred[]{:T(512)} %bitcast.17, f32[16,1,4,256]{3,0,2,1:T(8,128)S(1)} %convolution_bitcast_fusion.1), kind=kOutput, calls=%fused_computation.28 | convolution fusion | flops 134447104 | bytes 2949125 | tf_op jit(solution)/shard_map/glcf,lfd->glcd/dot_general | solution.py:183
  100.1 0.0 copy-start.5
  100.1 0.2 multiply_convert_fusion
  100.3 0.2 copy.167
  100.5 1.3 copy.153
  101.8 4.4 %all-to-all-start.2 = ((bf16[16,16,16,128]{3,1,2,0:T(8,128)(2,1)}), bf16[16,16,16,128]{3,1,2,0:T(8,128)(2,1)S(1)}, u32[]{:S(2)}, u32[]{:S(2)}) async-start(bf16[16,16,16,128]{3,1,2,0:T(8,128)(2,1)} %copy.153), calls=%async_computation.2 | async-start | bytes 2097152 | tf_op jit(solution)/shard_map/all_to_all | solution.py:45
  106.3 28.0 %all-to-all-done.2 = bf16[16,16,16,128]{3,1,2,0:T(8,128)(2,1)S(1)} async-done(((bf16[16,16,16,128]{3,1,2,0:T(8,128)(2,1)}), bf16[16,16,16,128]{3,1,2,0:T(8,128)(2,1)S(1)}, u32[]{:S(2)}, u32[]{:S(2)}) %all-to-all-start.2) | async-done | bytes 1048608 | tf_op jit(solution)/shard_map/all_to_all | solution.py:45
  134.3 0.1 reduce_sum.88
  134.4 0.6 copy.155
  135.1 3.5 %all-to-all-start.3 = ((bf16[16,16,128]{2,1,0:T(8,128)(2,1)}), bf16[16,16,128]{2,1,0:T(8,128)(2,1)S(1)}, u32[]{:S(2)}, u32[]{:S(2)}) async-start(bf16[16,16,128]{2,1,0:T(8,128)(2,1)} %copy.155), calls=%async_computation.3 | async-start | bytes 131072 | tf_op jit(solution)/shard_map/all_to_all | solution.py:194
  138.6 0.1 select_reduce_fusion
  138.7 6.3 %all-to-all-done.3 = bf16[16,16,128]{2,1,0:T(8,128)(2,1)S(1)} async-done(((bf16[16,16,128]{2,1,0:T(8,128)(2,1)}), bf16[16,16,128]{2,1,0:T(8,128)(2,1)S(1)}, u32[]{:S(2)}, u32[]{:S(2)}) %all-to-all-start.3) | async-done | bytes 65568 | tf_op jit(solution)/shard_map/all_to_all | solution.py:194
  145.0 0.8 fusion.11
  (18 shorter events, 0.2 us)
Async XLA Ops:
  0.6 97.4 %copy-start = (bf16[1,256,2048]{2,1,0:T(8,128)(2,1)S(1)}, bf16[1,256,2048]{2,1,0:T(8,128)(2,1)}, u32[]{:S(2)}) copy-start(bf16[1,256,2048]{2,1,0:T(8,128)(2,1)} %param.35) | copy-start | bytes 3145732
  0.6 44.7 %copy-start.7 = (f32[2048]{0:T(1024)S(1)}, f32[2048]{0:T(1024)}, u32[]{:S(2)}) copy-start(f32[2048]{0:T(1024)} %param.20) | copy-start | bytes 24580
  0.7 43.6 %copy-start.1 = (f32[64,4,256]{2,1,0:T(4,128)S(1)}, f32[64,4,256]{2,1,0:T(4,128)}, u32[]{:S(2)}) copy-start(f32[64,4,256]{2,1,0:T(4,128)} %param.31) | copy-start | bytes 786436
  25.1 26.1 %copy-start.3 = (f32[64,4]{0,1:T(4,128)}, f32[64,4]{0,1:T(4,128)S(1)}, u32[]{:S(2)}) copy-start(f32[64,4]{0,1:T(4,128)S(1)} %get-tuple-element.20) | copy-start | bytes 3076
  46.7 4.6 %copy-start.6 = (bf16[2048,4,16]{0,2,1:T(8,128)(2,1)S(1)}, bf16[2048,4,16]{0,2,1:T(8,128)(2,1)}, u32[]{:S(2)}) copy-start(bf16[2048,4,16]{0,2,1:T(8,128)(2,1)} %param.25) | copy-start | bytes 786436
  46.7 10.3 %copy-start.4 = (s32[64,2]{0,1:T(2,128)S(1)}, s32[64,2]{0,1:T(2,128)}, u32[]{:S(2)}) copy-start(s32[64,2]{0,1:T(2,128)} %param.36) | copy-start | bytes 1540
  51.3 18.1 %copy-start.2 = (f32[2048]{0:T(1024)S(1)}, f32[2048]{0:T(1024)}, u32[]{:S(2)}) copy-start(f32[2048]{0:T(1024)} %param.21) | copy-start | bytes 24580
  52.6 13.3 %all-to-all-start = ((bf16[16,2,2048]{2,1,0:T(2,128)(2,1)}), bf16[16,2,2048]{2,1,0:T(2,128)(2,1)S(1)}, u32[]{:S(2)}, u32[]{:S(2)}) async-start(bf16[16,2,2048]{2,1,0:T(2,128)(2,1)} %reshape.211), calls=%async_computation | async-start | bytes 262144 | tf_op jit(solution)/shard_map/all_to_all | solution.py:31
  70.9 25.0 %all-to-all-start.1 = ((bf16[16,16,2048]{2,1,0:T(8,128)(2,1)}), bf16[16,16,2048]{2,1,0:T(8,128)(2,1)S(1)}, u32[]{:S(2)}, u32[]{:S(2)}) async-start(bf16[16,16,2048]{2,1,0:T(8,128)(2,1)} %bitcast.18), calls=%async_computation.1 | async-start | bytes 2097152 | tf_op jit(solution)/shard_map/all_to_all | solution.py:164
  100.1 6.2 %copy-start.5 = (f32[64,2]{0,1:T(2,128)S(1)}, f32[64,2]{0,1:T(2,128)}, u32[]{:S(2)}) copy-start(f32[64,2]{0,1:T(2,128)} %param.37) | copy-start | bytes 1540
  101.8 32.5 %all-to-all-start.2 = ((bf16[16,16,16,128]{3,1,2,0:T(8,128)(2,1)}), bf16[16,16,16,128]{3,1,2,0:T(8,128)(2,1)S(1)}, u32[]{:S(2)}, u32[]{:S(2)}) async-start(bf16[16,16,16,128]{3,1,2,0:T(8,128)(2,1)} %copy.153), calls=%async_computation.2 | async-start | bytes 2097152 | tf_op jit(solution)/shard_map/all_to_all | solution.py:45
  135.1 10.0 %all-to-all-start.3 = ((bf16[16,16,128]{2,1,0:T(8,128)(2,1)}), bf16[16,16,128]{2,1,0:T(8,128)(2,1)S(1)}, u32[]{:S(2)}, u32[]{:S(2)}) async-start(bf16[16,16,128]{2,1,0:T(8,128)(2,1)} %copy.155), calls=%async_computation.3 | async-start | bytes 131072 | tf_op jit(solution)/shard_map/all_to_all | solution.py:194
where the time goes:
time: 147 us; the launch traced here: 146 us
  waiting for transfers between devices  60.4 us (41%)
  blocking collectives  38.3 us (26%)
  starting transfers between devices  19.1 us (13%)
  matrix products  14.6 us (10%)
  other arithmetic  6.67 us (5%)
  local copies, waits for them, and re-layouts  5.64 us (4%)
    all_to_all x1, waiting for transfers between devices, sent_and_summed(): lax.all_to_all(cut_along(shard, dim, devices), axis, 0, 0, tiled=True)  28 us
    all_gather x1, blocking collectives, local(): full_rows = lax.all_gather(tokens, 'tp', axis=1, tiled=True)  22.4 us
    all_to_all x1, waiting for transfers between devices, local(): lax.all_to_all(buffer.reshape(group_count, local_experts * capacity, norm...  18.2 us
    all_gather x1, blocking collectives, gather_turned(): lax.all_gather(both, axis, axis=0, tiled=True)  15.9 us
    all_to_all x1, waiting for transfers between devices, from_everyone(): return lax.all_to_all(copies, axis, split_axis=0, concat_axis=0, tiled=True)  7.86 us
    all_to_all x1, starting transfers between devices, local(): lax.all_to_all(buffer.reshape(group_count, local_experts * capacity, norm...  6.76 us
    all_to_all x1, waiting for transfers between devices, local(): lax.all_to_all(outgoing, 'ep', split_axis=0, concat_axis=0, tiled=True)  6.35 us
    unnamed x1, other arithmetic  4.5 us
  transfers between devices with their start and end apart: 4, of which 4 were waited for; matrix products, arithmetic and copies ran while one was open for 1% of the time, Pallas kernels for 0%

commit v1 on v0

v1 whole, which is shorter than its diff:
```python
import jax
import jax.numpy as jnp
from jax import lax
from jax.experimental import pallas as pl
from jax.experimental.pallas import tpu as pltpu
from jax.sharding import PartitionSpec as P

MESH = pl.DeviceIdType.MESH
F32, BF16 = jnp.float32, jnp.bfloat16
eps = 1e-06
ROWS, WIDTH, NTP, NEP, HEADS, HDIM, CAP, SPLIT = 64, 2048, 16, 16, 4, 256, 4, 4


def nt(a, b):
    return lax.dot_general(a, b, (((1,), (1,)), ((), ())), preferred_element_type=F32)


def nn(a, b):
    return jnp.dot(a, b, preferred_element_type=F32)


def iota(shape, dim):
    return lax.broadcasted_iota(jnp.int32, shape, dim)


def body(
    tok, gain_m, gain_e, qw, kw, vw, ow, igw, fgw, bias, mixout, mem, norm, mstate, egate, eup, edown, rt, rw,
    mixed, kfull, vout, dec_out, inf_out, max_out,
    xg, wall, igs, fgs, wgf, gms, ges, memv, memb, normv, mixw, egv, euv, edv, sm, mss, rts, rws, perm, perm2,
    comb, pbt, pbf, nso, scaled, qkb, pb, gb, mid, nst, sbuf, rbuf, dbuf, zbuf, obuf, fbuf,
    lsem, ssem, rsem,
):
    ep, tp = lax.axis_index("ep"), lax.axis_index("tp")
    group, block = tp // SPLIT, tp % SPLIT

    def local(i, src, dst):
        return pltpu.make_async_copy(src, dst, lsem.at[i])

    loads = [
        local(0, tok, xg.at[tp]),
        local(1, rt, rts), local(2, rw, rws), local(3, mstate, mss),
        local(4, igw, igs), local(5, fgw, fgs), local(6, gain_m, gms), local(7, gain_e, ges),
        local(8, qw, wall.at[0:64]), local(9, kw, wall.at[64:128]),
        local(10, vw, wall.at[128:192]), local(11, ow, wall.at[192:256]),
        local(12, norm, normv), local(13, mem, memv),
    ]
    loads += [local(14 + h, mixout.at[h], mixw.at[:, h]) for h in range(HEADS)]
    loads += [local(18, egate, egv), local(19, eup, euv), local(20, edown, edv)]
    for c in loads:
        c.start()

    barrier = pltpu.get_barrier_semaphore()

    def greet(d, _):
        pl.semaphore_signal(barrier, inc=1, device_id=(ep, lax.rem(tp + d, NTP)), device_id_type=MESH)
        pl.semaphore_signal(barrier, inc=1, device_id=(lax.rem(ep + d, NEP), tp), device_id_type=MESH)
        return 0

    lax.fori_loop(1, 16, greet, 0)

    i, j = iota((256, 256), 0), iota((256, 256), 1)
    perm[...] = (j == (((i >> 2) & 15) << 4) + ((i >> 6) << 2) + (i & 3)).astype(F32).astype(BF16)
    i, c = iota((256, 1024), 0), iota((256, 1024), 1)
    perm2[...] = (
        (((c >> 8) == ((i >> 2) & 3)) & ((c & 63) == ((i >> 4) << 2) + (i & 3))).astype(F32).astype(BF16)
    )

    pl.semaphore_wait(barrier, 30)

    def over_tp(phase, src, dst, peer_of_src):
        def copy(d):
            peer = lax.rem(tp + d, NTP)
            return pltpu.make_async_remote_copy(
                src_ref=src(peer), dst_ref=dst(tp), send_sem=ssem.at[phase, peer], recv_sem=rsem.at[phase, tp],
                device_id=(ep, peer), device_id_type=MESH)
        return copy

    def over_ep(phase, src, dst):
        def copy(d):
            peer = lax.rem(ep + d, NEP)
            return pltpu.make_async_remote_copy(
                src_ref=src(peer), dst_ref=dst(ep), send_sem=ssem.at[phase, peer], recv_sem=rsem.at[phase, ep],
                device_id=(peer, tp), device_id_type=MESH)
        return copy

    def start_all(copy):
        def step(d, _):
            copy(d).start()
            return 0
        lax.fori_loop(1, 16, step, 0)

    def sent_all(copy):
        def step(d, _):
            copy(d).wait_send()
            return 0
        lax.fori_loop(1, 16, step, 0)

    def arrived(phase, dst, me, axis_pos):
        def step(d, _):
            peer = lax.rem(me + d, 16)
            pltpu.make_async_remote_copy(
                src_ref=dst(peer), dst_ref=dst(peer), send_sem=ssem.at[phase, peer], recv_sem=rsem.at[phase, peer],
                device_id=axis_pos(peer), device_id_type=MESH).wait_recv()
            return 0
        lax.fori_loop(1, 16, step, 0)

    def tp_pos(peer):
        return (ep, peer)

    def ep_pos(peer):
        return (peer, tp)

    send_tok = over_tp(0, lambda p: xg.at[tp], lambda me: xg.at[me], None)
    send_qk = over_tp(1, lambda p: qkb.at[tp], lambda me: qkb.at[me], None)
    send_pb = over_tp(2, lambda p: pb.at[tp], lambda me: pb.at[me], None)
    send_g = over_tp(3, lambda p: gb.at[tp], lambda me: gb.at[me], None)
    send_rows = over_ep(4, lambda p: sbuf.at[p], lambda me: rbuf.at[me])
    send_z = over_tp(5, lambda p: dbuf.at[p], lambda me: zbuf.at[me], None)
    send_f = over_ep(6, lambda p: obuf.at[p], lambda me: fbuf.at[me])

    loads[0].wait()
    start_all(send_tok)

    for c in loads[1:8]:
        c.wait()
    sm[...] = jnp.zeros((128, 128), F32)
    sm[0:4, 0:64] = mss[...]
    sm[4:6, 0:64] = rws[...]
    sm[6:8, 0:64] = rts[...].astype(F32)
    cols = jnp.transpose(sm[...])[0:ROWS]
    w0, w1, r0, r1 = cols[:, 4:5], cols[:, 5:6], cols[:, 6:7], cols[:, 7:8]
    total = w0 + w1
    before = (iota((ROWS, ROWS), 1) < iota((ROWS, ROWS), 0)).astype(F32).astype(BF16)
    lane = iota((ROWS, 256), 1)
    slot_of = (lane & 3).astype(F32)
    expert = (lane >> 2).astype(F32)
    zero = jnp.zeros((ROWS, 256), F32)
    named0, named1 = r0 == expert, r1 == expert
    hit = jnp.where(named0 | named1, 1.0, zero)
    share = jnp.where(named0, w0 / total, zero) + jnp.where(named1, w1 / total, zero)
    share = jnp.where(nn(before, hit.astype(BF16)) == slot_of, share, zero)
    high = share.astype(BF16)
    comb[0:64] = high
    comb[64:128] = (share - high.astype(F32)).astype(BF16)
    expert = ((lane >> 4) * SPLIT + group).astype(F32)
    hit = jnp.where((r0 == expert) | (r1 == expert), 1.0, zero)
    pick = jnp.where(nn(before, hit.astype(BF16)) == slot_of, hit, zero)
    quarter = (lane >> 2) & 3
    for q in range(4):
        pbf[q * 64 : (q + 1) * 64] = jnp.where(quarter == q, pick, zero)
    pbt[...] = jnp.transpose(pbf[...]).astype(BF16)

    wgf[...] = jnp.zeros((16, WIDTH), F32)
    wgf[0:4] = igs[...].astype(F32)
    wgf[4:8] = fgs[...].astype(F32)
    wall[256:384] = jnp.zeros((128, WIDTH), BF16)
    wall[256:272] = wgf[...].astype(BF16)
    for c in loads[8:14]:
        c.wait()

    def narrow(k, _):
        at = pl.multiple_of(k * 8, 8)
        to = pl.multiple_of(k * 128, 128)
        for h in range(HEADS):
            memb[h, pl.ds(to, 128), :] = memv[pl.ds(at, 8), h].reshape(128, HDIM).astype(BF16)
        return 0

    lax.fori_loop(0, 8, narrow, 0)

    place = jnp.full((ROWS, 128), tp, jnp.int32)
    chosen = jnp.zeros((ROWS, 128), F32)
    for half in range(8):
        piece = normv[:, half // 2, (half % 2) * 128 : (half % 2 + 1) * 128]
        chosen = jnp.where(place >> 1 == half, piece, chosen)
    nso[...] = jnp.where((place & 1) == 1, pltpu.roll(chosen, 64, 1), chosen)

    arrived(0, lambda p: xg.at[p], tp, tp_pos)
    square = jnp.zeros((ROWS, 128), F32)
    for b in range(NTP):
        x = xg[b].astype(F32)
        square += x * x
        scaled[:, b * 128 : (b + 1) * 128] = (x * gms[b : b + 1, :]).astype(BF16)
    inverse = lax.rsqrt(jnp.sum(square, axis=1, keepdims=True) * (1.0 / WIDTH) + eps)
    acc = nt(scaled[...], wall[...]) * inverse
    lanes = iota((ROWS, 128), 1)
    low = lanes < 64
    qk = acc[:, 0:128] * jnp.where(low, 1.0, HDIM ** (-0.5))
    qkb[tp] = qk.astype(BF16)
    start_all(send_qk)
    ns = nso[...]
    dot_n = jnp.sum(jnp.where(low, qk * ns, 0.0), axis=1, keepdims=True)
    dot_k = jnp.sum(jnp.where(low, qk * pltpu.roll(qk, 64, 1), 0.0), axis=1, keepdims=True)
    sm[0:64] = jnp.where(lanes == 0, dot_n, jnp.where(lanes == 1, dot_k, 0.0))
    pb[tp] = jnp.transpose(sm[...])[0:8]
    start_all(send_pb)

    vo = acc[:, 128:256]
    values = jnp.where(low, vo, pltpu.roll(vo, 64, 1))
    outgate = jnp.where(low, pltpu.roll(vo, 64, 1), vo)
    opened = jax.nn.sigmoid(outgate)
    ga = acc[:, 256:384]
    ingate = ga[:, 0:4]
    pre = pltpu.roll(ga, 124, 1)[:, 0:4] + bias[...]
    logforget = -(jnp.maximum(-pre, 0.0) + jnp.log1p(jnp.exp(-jnp.abs(pre))))
    carried = logforget + cols[:, 0:4]
    max_next = jnp.maximum(carried, ingate)
    decay = jnp.exp(carried - max_next)
    inflow = jnp.exp(ingate - max_next)
    floor = jnp.exp(-max_next)
    max_out[...] = max_next
    dec_out[...] = decay
    inf_out[...] = inflow
    vout[...] = values
    head = (lanes >> 4) & 3

    def spread(columns):
        out = jnp.broadcast_to(columns[0], (ROWS, 128))
        for h in range(1, HEADS):
            out = jnp.where(head == h, columns[h], out)
        return out

    def by_head(a):
        return [a[:, h : h + 1] for h in range(HEADS)]

    arrived(1, lambda p: qkb.at[p], tp, tp_pos)
    numerator = jnp.zeros((ROWS, 128), F32)
    own = (lanes >> 4) == (iota((ROWS, 128), 0) & 7)
    for h in range(HEADS):
        q_parts = []
        for s in range(2):
            a, b = qkb[4 * h + 2 * s].astype(F32), qkb[4 * h + 2 * s + 1].astype(F32)
            q_parts.append(jnp.where(low, a, pltpu.roll(b, 64, 1)).astype(BF16))
            kfull[:, h * 256 + s * 128 : h * 256 + (s + 1) * 128] = jnp.where(low, pltpu.roll(a, 64, 1), b).astype(BF16)
        q = jnp.concatenate(q_parts, axis=1)
        pieces = []
        for t in range(4):
            r = nt(q[t * 16 : (t + 1) * 16], memb[h, t * 256 : (t + 1) * 256])
            pieces += [r[0:8, 0:128], r[8:16, 128:256]]
        diagonal = jnp.where(own, jnp.concatenate(pieces, axis=0), 0.0)
        for shift in (64, 32, 16):
            diagonal = diagonal + pltpu.roll(diagonal, shift, 1)
        numerator = jnp.where(head == h, diagonal, numerator)
    arrived(2, lambda p: pb.at[p], tp, tp_pos)
    for h in range(HEADS):
        sm[h * 8 : (h + 1) * 8] = (pb[4 * h] + pb[4 * h + 1]) + (pb[4 * h + 2] + pb[4 * h + 3])
    sums = jnp.transpose(sm[...])[0:ROWS]
    with_n = spread([sums[:, 8 * h : 8 * h + 1] for h in range(HEADS)])
    with_k = spread([sums[:, 8 * h + 1 : 8 * h + 2] for h in range(HEADS)])
    decay_l, inflow_l, floor_l = spread(by_head(decay)), spread(by_head(inflow)), spread(by_head(floor))
    denominator = jnp.maximum(jnp.abs(decay_l * with_n + inflow_l * with_k), floor_l)
    recall = (decay_l * numerator + inflow_l * values * with_k) / denominator
    gated = opened * recall
    gb[tp] = jnp.where(low[0:32], gated[0:32], gated[32:64]).astype(BF16)
    start_all(send_g)

    for c in loads[14:]:
        c.wait()
    arrived(3, lambda p: gb.at[p], tp, tp_pos)
    tops, ends = [], []
    low32 = low[0:32]
    for s in range(8):
        a, b = gb[2 * s].astype(F32), gb[2 * s + 1].astype(F32)
        tops.append(jnp.where(low32, a, pltpu.roll(b, 64, 1)).astype(BF16))
        ends.append(jnp.where(low32, pltpu.roll(a, 64, 1), b).astype(BF16))
    heads = jnp.concatenate([jnp.concatenate(tops, axis=1), jnp.concatenate(ends, axis=1)], axis=0)
    square = jnp.zeros((ROWS, 128), F32)
    for n in range(4):
        part = nn(heads, mixw[:, :, :, n * 512 : (n + 1) * 512].reshape(1024, 512))
        for b in range(4):
            m = (xg[4 * n + b].astype(F32) + part[:, b * 128 : (b + 1) * 128]).astype(BF16)
            mid[4 * n + b] = m
            m = m.astype(F32)
            square += m * m
    inverse = lax.rsqrt(jnp.sum(square, axis=1, keepdims=True) * (1.0 / WIDTH) + eps)
    for b in range(NTP):
        nst[(b // 4) * 64 : (b // 4 + 1) * 64, (b % 4) * 128 : (b % 4 + 1) * 128] = (
            mid[b].astype(F32) * inverse * ges[b : b + 1, :]
        ).astype(BF16)
    sbuf[...] = nn(pbt[...], nst[...]).astype(BF16).reshape(NEP, 16, 512)
    start_all(send_rows)
    rbuf[ep] = sbuf[ep]

    arrived(4, lambda p: rbuf.at[p], ep, ep_pos)
    rows = nn(perm[...], rbuf[...].reshape(256, 512)).astype(BF16)
    gate = jnp.zeros((ROWS, 256), F32)
    up = jnp.zeros((ROWS, 256), F32)
    for q in range(4):
        r = rows[q * 64 : (q + 1) * 64]
        gate += nn(r, egv[0, q * 512 : (q + 1) * 512, :])
        up += nn(r, euv[0, q * 512 : (q + 1) * 512, :])
    hidden = (gate * jax.nn.sigmoid(gate) * up).astype(BF16)
    for n in range(4):
        part = nn(hidden, edv[0, :, n * 512 : (n + 1) * 512]).astype(BF16)
        for b in range(4):
            dbuf[4 * n + b] = part[:, b * 128 : (b + 1) * 128]
    start_all(send_z)
    zbuf[tp] = dbuf[tp]
    arrived(5, lambda p: zbuf.at[p], tp, tp_pos)
    obuf[...] = nn(perm2[...], zbuf[...].reshape(1024, 128)).astype(BF16).reshape(NEP, 16, 128)
    start_all(send_f)
    fbuf[ep] = obuf[ep]
    arrived(6, lambda p: fbuf.at[p], ep, ep_pos)
    both = nn(comb[...], fbuf[...].reshape(256, 128))
    mixed[...] = (mid[tp].astype(F32) + (both[0:64] + both[64:128])).astype(BF16)
    for copy in (send_tok, send_qk, send_pb, send_g, send_rows, send_z, send_f):
        sent_all(copy)


def local(
    tokens, mixer_gain, expert_gain, query_weight, key_weight, value_weight, outgate_weight, ingate_weight,
    forget_weight, forget_bias, mixout_weight, memory_state, norm_state, max_state, expert_gate, expert_up,
    expert_down, routes, route_weights,
):
    hbm = pl.BlockSpec(memory_space=pl.ANY)
    vm = pl.BlockSpec(memory_space=pltpu.VMEM)
    scratch = [
        pltpu.VMEM((NTP, ROWS, 128), BF16),
        pltpu.VMEM((384, WIDTH), BF16),
        pltpu.VMEM((4, WIDTH), BF16), pltpu.VMEM((4, WIDTH), BF16),
        pltpu.VMEM((16, WIDTH), F32),
        pltpu.VMEM((16, 128), F32), pltpu.VMEM((16, 128), F32),
        pltpu.VMEM((ROWS, HEADS, 16, HDIM), F32),
        pltpu.VMEM((HEADS, 1024, HDIM), BF16),
        pltpu.VMEM((ROWS, HEADS, HDIM), F32),
        pltpu.VMEM((NTP, HEADS, 16, WIDTH), BF16),
        pltpu.VMEM((1, WIDTH, 256), BF16), pltpu.VMEM((1, WIDTH, 256), BF16), pltpu.VMEM((1, 256, WIDTH), BF16),
        pltpu.VMEM((128, 128), F32),
        pltpu.VMEM((4, 64), F32), pltpu.VMEM((2, 64), jnp.int32), pltpu.VMEM((2, 64), F32),
        pltpu.VMEM((256, 256), BF16), pltpu.VMEM((256, 1024), BF16),
        pltpu.VMEM((128, 256), BF16), pltpu.VMEM((256, 256), BF16), pltpu.VMEM((256, 256), F32),
        pltpu.VMEM((ROWS, 128), F32),
        pltpu.VMEM((ROWS, WIDTH), BF16),
        pltpu.VMEM((NTP, ROWS, 128), BF16), pltpu.VMEM((NTP, 8, 128), F32),
        pltpu.VMEM((NTP, 32, 128), BF16),
        pltpu.VMEM((NTP, ROWS, 128), BF16), pltpu.VMEM((256, 512), BF16),
        pltpu.VMEM((NEP, 16, 512), BF16), pltpu.VMEM((NEP, 16, 512), BF16),
        pltpu.VMEM((NTP, ROWS, 128), BF16), pltpu.VMEM((NTP, ROWS, 128), BF16),
        pltpu.VMEM((NEP, 16, 128), BF16), pltpu.VMEM((NEP, 16, 128), BF16),
        pltpu.SemaphoreType.DMA((21,)), pltpu.SemaphoreType.DMA((7, 16)), pltpu.SemaphoreType.DMA((7, 16)),
    ]
    mixed, kfull, vals, decay, inflow, max_next = pl.pallas_call(
        body,
        out_shape=[
            jax.ShapeDtypeStruct((ROWS, 128), BF16),
            jax.ShapeDtypeStruct((ROWS, 1024), BF16),
            jax.ShapeDtypeStruct((ROWS, 128), F32),
            jax.ShapeDtypeStruct((ROWS, HEADS), F32),
            jax.ShapeDtypeStruct((ROWS, HEADS), F32),
            jax.ShapeDtypeStruct((ROWS, HEADS), F32),
        ],
        in_specs=[hbm] * 9 + [vm] + [hbm] * 9,
        out_specs=[vm] * 6,
        scratch_shapes=scratch,
        compiler_params=pltpu.CompilerParams(
            collective_id=0, has_side_effects=True, vmem_limit_bytes=40 * 1024 * 1024
        ),
        name="step",
    )(
        tokens, mixer_gain.reshape(16, 128), expert_gain.reshape(16, 128),
        query_weight.T, key_weight.T,
        value_weight.transpose(1, 2, 0).reshape(64, WIDTH), outgate_weight.transpose(1, 2, 0).reshape(64, WIDTH),
        ingate_weight.T, forget_weight.T, forget_bias.reshape(1, HEADS),
        mixout_weight.reshape(HEADS, NTP, 16, WIDTH),
        memory_state, norm_state, max_state.T, expert_gate, expert_up, expert_down, routes.T, route_weights.T,
    )
    keys = kfull.reshape(ROWS, HEADS, HDIM).astype(F32)
    v = vals[:, 0:64].reshape(ROWS, HEADS, 16)
    memory_next = (
        decay[:, :, None, None] * memory_state + (inflow[:, :, None] * v)[:, :, :, None] * keys[:, :, None, :]
    )
    norm_next = decay[:, :, None] * norm_state + inflow[:, :, None] * keys
    return (mixed, memory_next, norm_next, max_next)


def solution(mesh):
    in_specs = (
        P("ep", "tp"), P(), P(), P(None, "tp"), P(None, "tp"), P(None, None, "tp"), P(None, None, "tp"), P(), P(), P(),
        P(), P("ep", None, "tp", None), P("ep", None, None), P("ep", None), P(("ep", "tp"), None, None),
        P(("ep", "tp"), None, None), P(("ep", "tp"), None, None), P("ep", None), P("ep", None),
    )
    out_specs = (P("ep", "tp"), P("ep", None, "tp", None), P("ep", None, None), P("ep", None))
    return jax.shard_map(local, mesh=mesh, in_specs=in_specs, out_specs=out_specs, check_vma=False)
```

time: 147 us -> 89.6 us (0.61)
  Pallas kernels: 0 us -> 62.4 us
  waiting for transfers between devices: 60.4 us -> 0 us
  blocking collectives: 38.3 us -> 0 us
  starting transfers between devices: 19.1 us -> 0 us
  local copies, waits for them, and re-layouts: 5.64 us -> 20.7 us
  matrix products: 14.6 us -> 0 us
  other arithmetic: 6.67 us -> 5.05 us
    pallas_call x0 -> x1, Pallas kernels: none -> 62.4 us  [local(): pl.pallas_call(body, out_shape=[jax.ShapeDtypeStruct((ROWS, 128), BF16),...]
    all_to_all x4 -> x0, waiting for transfers between devices: 60.4 us -> none  [the longest x1 28 us: sent_and_summed(): lax.all_to_all(cut_along(shard, dim, devices), axis, 0, 0, tiled=True)]
    all_gather x2 -> x0, blocking collectives: 38.3 us -> none  [the longest x1 22.4 us: local(): full_rows = lax.all_gather(tokens, 'tp', axis=1, tiled=True)]
    all_to_all x4 -> x0, starting transfers between devices: 19.1 us -> none  [the longest x1 6.76 us: local(): lax.all_to_all(buffer.reshape(group_count, local_experts * capacity, norm...]
    unnamed x22 -> x42, local copies, waits for them, and re-layouts: 1.71 us -> 20.3 us
    dot_general x11 -> x0, matrix products: 14.6 us -> none  [the longest x1 3.17 us: local(): jnp.dot(heads_full, mixout_weight, preferred_element_type=jnp.float32)]
    add x1 -> x2, other arithmetic: 0.01 us -> 5.04 us  [the longest x1 4.13 us: local(): decay[:, :, None, None] * memory_state]
    unnamed x1 -> x0, other arithmetic: 4.5 us -> none
  transfers between devices with their start and end apart: 4 -> 0, of which waited for: 4 -> 0; matrix products, arithmetic and copies ran while one was open for 1% -> 0% of each run, Pallas kernels for 0% -> 0%
where the time goes in v1:
time: 89.6 us; the launch traced here: 88.8 us
  Pallas kernels  62.4 us (70%)
  local copies, waits for them, and re-layouts  20.7 us (23%)
  other arithmetic  5.05 us (6%)
    pallas_call x1, Pallas kernels, local(): pl.pallas_call(body, out_shape=[jax.ShapeDtypeStruct((ROWS, 128), BF16),...  62.4 us
    unnamed x42, local copies, waits for them, and re-layouts  20.3 us
    add x1, other arithmetic, local(): decay[:, :, None, None] * memory_state  4.13 us

profile of v1, /device:TPU:1, one launch (start us, length us, event | category | flops | bytes accessed | tf_op | source)
XLA Modules:
  0.0 88.8 jit_solution(3982327179246850784)
XLA Ops:
  0.6 0.0 copy-start
  0.7 2.2 %copy-done = f32[64,4,16,256]{3,2,1,0:T(8,128)S(1)} copy-done((f32[64,4,16,256]{3,2,1,0:T(8,128)S(1)}, f32[64,4,16,256]{3,2,1,0:T(8,128)}, u32[]{:S(2)}) %copy-start) | copy-done | bytes 4194328
  2.8 0.0 copy-start.1
  2.8 2.2 %copy-done.1 = bf16[1024,2048]{1,0:T(8,128)(2,1)S(1)} copy-done((bf16[1024,2048]{1,0:T(8,128)(2,1)S(1)}, bf16[1024,2048]{1,0:T(8,128)(2,1)}, u32[]{:S(2)}) %copy-start.1) | copy-done | bytes 4194328
  5.0 0.0 copy-start.2
  5.0 1.2 %copy-done.2 = bf16[1,2048,256]{2,1,0:T(8,128)(2,1)S(1)} copy-done((bf16[1,2048,256]{2,1,0:T(8,128)(2,1)S(1)}, bf16[1,2048,256]{2,1,0:T(8,128)(2,1)}, u32[]{:S(2)}) %copy-start.2) | copy-done | bytes 1048600
  6.2 0.0 copy-start.3
  6.2 1.2 %copy-done.3 = bf16[1,2048,256]{2,1,0:T(8,128)(2,1)S(1)} copy-done((bf16[1,2048,256]{2,1,0:T(8,128)(2,1)S(1)}, bf16[1,2048,256]{2,1,0:T(8,128)(2,1)}, u32[]{:S(2)}) %copy-start.3) | copy-done | bytes 1048600
  7.5 0.0 copy-start.4
  7.5 1.2 %copy-done.4 = bf16[1,256,2048]{2,1,0:T(8,128)(2,1)S(1)} copy-done((bf16[1,256,2048]{2,1,0:T(8,128)(2,1)S(1)}, bf16[1,256,2048]{2,1,0:T(8,128)(2,1)}, u32[]{:S(2)}) %copy-start.4) | copy-done | bytes 1048600
  8.7 0.0 copy-start.5
  8.7 0.9 %copy-done.5 = f32[64,4,256]{2,1,0:T(4,128)S(1)} copy-done((f32[64,4,256]{2,1,0:T(4,128)S(1)}, f32[64,4,256]{2,1,0:T(4,128)}, u32[]{:S(2)}) %copy-start.5) | copy-done | bytes 262168
  9.6 0.0 copy-start.7
  9.6 0.9 %copy-done.7 = bf16[2048,64]{0,1:T(8,128)(2,1)S(1)} copy-done((bf16[2048,64]{0,1:T(8,128)(2,1)S(1)}, bf16[2048,64]{0,1:T(8,128)(2,1)}, u32[]{:S(2)}) %copy-start.7) | copy-done | bytes 262168
  10.6 0.0 copy-start.8
  10.6 0.9 %copy-done.8 = bf16[2048,64]{0,1:T(8,128)(2,1)S(1)} copy-done((bf16[2048,64]{0,1:T(8,128)(2,1)S(1)}, bf16[2048,64]{0,1:T(8,128)(2,1)}, u32[]{:S(2)}) %copy-start.8) | copy-done | bytes 262168
  11.5 0.0 copy-start.9
  11.5 0.9 %copy-done.9 = bf16[2048,4,16]{0,2,1:T(8,128)(2,1)S(1)} copy-done((bf16[2048,4,16]{0,2,1:T(8,128)(2,1)S(1)}, bf16[2048,4,16]{0,2,1:T(8,128)(2,1)}, u32[]{:S(2)}) %copy-start.9) | copy-done | bytes 262168
  12.5 0.0 copy-start.10
  12.5 0.9 %copy-done.10 = bf16[2048,4,16]{0,2,1:T(8,128)(2,1)S(1)} copy-done((bf16[2048,4,16]{0,2,1:T(8,128)(2,1)S(1)}, bf16[2048,4,16]{0,2,1:T(8,128)(2,1)}, u32[]{:S(2)}) %copy-start.10) | copy-done | bytes 262168
  13.4 0.0 copy-start.11
  13.4 0.7 copy-done.11
  14.2 0.0 copy-start.12
  14.2 0.7 copy-done.12
  14.9 0.0 copy-start.13
  14.9 0.7 copy-done.13
  15.6 0.0 copy-start.14
  15.6 0.7 copy-done.14
  16.3 0.0 copy-start.15
  16.3 0.7 copy-done.15
  17.0 0.0 copy-start.16
  17.0 0.7 copy-done.16
  17.7 0.0 copy-start.17
  17.7 0.7 copy-done.17
  18.4 0.0 copy-start.18
  18.4 0.7 copy-done.18
  19.0 0.0 copy-start.19
  19.0 0.7 copy-done.19
  19.7 62.4 %step.1 = (bf16[64,128]{1,0:T(8,128)(2,1)S(1)}, bf16[64,1024]{1,0:T(8,128)(2,1)S(1)}, f32[64,128]{1,0:T(8,128)S(1)}, f32[64,4]{1,0:T(8,128)S(1)}, f32[64,4]{1,0:T(8,128)S(1)}, /*index=5*/f32[64,4]{1,0:T(8,128)S(1)}) custom-call(bf16[64,128]{1,0:T(8,128)(2,1)S(1)} %copy-done.11, f32[16,128]{1,0:T(8,128)S(1)} %bitcast.27, f32[16,128]{1,0:T(8,128)S(1)} %bitcast.28, ...), custom_call_target="tpu_custom_call" | custom-call | tf_op jit(solution)/shard_map/step/pallas_call | solution.py:341
  82.1 0.1 copy.24
  82.2 0.1 copy.25
  82.3 0.1 copy.26
  82.4 0.1 reshape.52
  82.5 0.0 copy-start.6
  82.5 4.1 %multiply_add_fusion = f32[64,4,16,256]{3,2,1,0:T(8,128)} fusion(f32[64,4,16,256]{3,2,1,0:T(8,128)} %mem.1, f32[64,4,256]{2,1,0:T(4,128)S(1)} %reshape.52, f32[64,4,16]{2,1,0:T(4,128)S(1)} %copy.26, f32[64,4]{1,0:T(8,128)S(1)} %get-tuple-element.11), kind=kLoop, calls=%fused_computation | loop fusion | flops 3145728 | bytes 8668160 | tf_op jit(solution)/shard_map/add | solution.py:369
  86.6 0.0 copy-done.6
  86.6 0.9 %multiply_add_fusion.1 = f32[64,4,256]{2,1,0:T(4,128)} fusion(f32[64,4,256]{2,1,0:T(4,128)S(1)} %reshape.52, f32[64,4,256]{2,1,0:T(4,128)S(1)} %copy-done.6, f32[64,4]{1,0:T(8,128)S(1)} %get-tuple-element.12, f32[64,4]{1,0:T(8,128)S(1)} %get-tuple-element.11), kind=kLoop, calls=%fused_computation.1 | loop fusion | flops 196608 | bytes 788480 | tf_op jit(solution)/shard_map/add | solution.py:371
  87.6 0.7 copy.27
  88.2 0.6 copy.29
  (1 shorter events, 0.0 us)
Async XLA Ops:
  0.6 2.2 %copy-start = (f32[64,4,16,256]{3,2,1,0:T(8,128)S(1)}, f32[64,4,16,256]{3,2,1,0:T(8,128)}, u32[]{:S(2)}) copy-start(f32[64,4,16,256]{3,2,1,0:T(8,128)} %mem.1) | copy-start | bytes 12582916
  2.8 2.2 %copy-start.1 = (bf16[1024,2048]{1,0:T(8,128)(2,1)S(1)}, bf16[1024,2048]{1,0:T(8,128)(2,1)}, u32[]{:S(2)}) copy-start(bf16[1024,2048]{1,0:T(8,128)(2,1)} %param.29) | copy-start | bytes 12582916
  5.0 1.2 %copy-start.2 = (bf16[1,2048,256]{2,1,0:T(8,128)(2,1)S(1)}, bf16[1,2048,256]{2,1,0:T(8,128)(2,1)}, u32[]{:S(2)}) copy-start(bf16[1,2048,256]{2,1,0:T(8,128)(2,1)} %egate.1) | copy-start | bytes 3145732
  6.2 1.2 %copy-start.3 = (bf16[1,2048,256]{2,1,0:T(8,128)(2,1)S(1)}, bf16[1,2048,256]{2,1,0:T(8,128)(2,1)}, u32[]{:S(2)}) copy-start(bf16[1,2048,256]{2,1,0:T(8,128)(2,1)} %eup.1) | copy-start | bytes 3145732
  7.5 1.2 %copy-start.4 = (bf16[1,256,2048]{2,1,0:T(8,128)(2,1)S(1)}, bf16[1,256,2048]{2,1,0:T(8,128)(2,1)}, u32[]{:S(2)}) copy-start(bf16[1,256,2048]{2,1,0:T(8,128)(2,1)} %edown.1) | copy-start | bytes 3145732
  8.7 0.9 %copy-start.5 = (f32[64,4,256]{2,1,0:T(4,128)S(1)}, f32[64,4,256]{2,1,0:T(4,128)}, u32[]{:S(2)}) copy-start(f32[64,4,256]{2,1,0:T(4,128)} %norm.1) | copy-start | bytes 786436
  9.6 0.9 %copy-start.7 = (bf16[2048,64]{0,1:T(8,128)(2,1)S(1)}, bf16[2048,64]{0,1:T(8,128)(2,1)}, u32[]{:S(2)}) copy-start(bf16[2048,64]{0,1:T(8,128)(2,1)} %param.22) | copy-start | bytes 786436
  10.6 0.9 %copy-start.8 = (bf16[2048,64]{0,1:T(8,128)(2,1)S(1)}, bf16[2048,64]{0,1:T(8,128)(2,1)}, u32[]{:S(2)}) copy-start(bf16[2048,64]{0,1:T(8,128)(2,1)} %param.23) | copy-start | bytes 786436
  11.5 0.9 %copy-start.9 = (bf16[2048,4,16]{0,2,1:T(8,128)(2,1)S(1)}, bf16[2048,4,16]{0,2,1:T(8,128)(2,1)}, u32[]{:S(2)}) copy-start(bf16[2048,4,16]{0,2,1:T(8,128)(2,1)} %param.24) | copy-start | bytes 786436
  12.5 0.9 %copy-start.10 = (bf16[2048,4,16]{0,2,1:T(8,128)(2,1)S(1)}, bf16[2048,4,16]{0,2,1:T(8,128)(2,1)}, u32[]{:S(2)}) copy-start(bf16[2048,4,16]{0,2,1:T(8,128)(2,1)} %param.25) | copy-start | bytes 786436
  13.4 0.7 copy-start.11
  14.2 0.7 copy-start.12
  14.9 0.7 copy-start.13
  15.6 0.7 copy-start.14
  16.3 0.7 copy-start.15
  17.0 0.7 copy-start.16
  17.7 0.7 copy-start.17
  18.4 0.7 copy-start.18
  19.0 0.7 copy-start.19
  82.5 4.1 %copy-start.6 = (f32[64,4,256]{2,1,0:T(4,128)S(1)}, f32[64,4,256]{2,1,0:T(4,128)}, u32[]{:S(2)}) copy-start(f32[64,4,256]{2,1,0:T(4,128)} %norm.1) | copy-start | bytes 786436

commit v2 on v1

v2 whole, which is shorter than its diff:
```python
import jax
import jax.numpy as jnp
from jax import lax
from jax.experimental import pallas as pl
from jax.experimental.pallas import tpu as pltpu
from jax.sharding import PartitionSpec as P

MESH = pl.DeviceIdType.MESH
F32, BF16 = jnp.float32, jnp.bfloat16
eps = 1e-06
ROWS, WIDTH, NTP, NEP, HEADS, HDIM, CAP, SPLIT = 64, 2048, 16, 16, 4, 256, 4, 4


def nt(a, b):
    return lax.dot_general(a, b, (((1,), (1,)), ((), ())), preferred_element_type=F32)


def nn(a, b):
    return jnp.dot(a, b, preferred_element_type=F32)


def iota(shape, dim):
    return lax.broadcasted_iota(jnp.int32, shape, dim)


FAR_EP = sorted(((dy, dx) for dy in range(4) for dx in range(4) if dy or dx), key=lambda p: (-(min(p[0], 4 - p[0]) + min(p[1], 4 - p[1])), p))
FAR_Z = (4, 3, 5, 2, 6, 1, 7)


def body(
    tok, gain_m, gain_e, qw, kw, vw, ow, igw, fgw, bias, mixout, mem, norm, mstate, egate, eup, edown, rt, rw,
    mixed, keys_out, update_out, decay_out, norm_out, max_out,
    xg, wall, igs, fgs, wgf, gms, ges, memv, memb, normv, mixw, egv, euv, edv, sm, mss, rts, rws, perm, perm2,
    comb, pbt, pbf, nso, scaled, qb, kb, pb, gb, mid, nst, sbuf, rbuf, half32, half16, pair, zsend, zbuf, obuf, fbuf,
    keys, upt, det, mxt, mixv,
    lsem, ssem, fsem, rsem, psem, osem,
):
    ep, tp = lax.axis_index("ep"), lax.axis_index("tp")
    group, chip, core = tp // SPLIT, tp // 2, tp % 2
    other = chip * 2 + (1 - core)
    ey, ex = ep // 4, ep % 4

    def local(i, src, dst):
        return pltpu.make_async_copy(src, dst, lsem.at[i])

    loads = [
        local(0, tok, xg.at[tp]),
        local(1, rt, rts), local(2, rw, rws), local(3, mstate, mss),
        local(4, igw, igs), local(5, fgw, fgs), local(6, gain_m, gms), local(7, gain_e, ges),
        local(8, qw, wall.at[0:64]), local(9, kw, wall.at[64:128]),
        local(10, vw, wall.at[128:192]), local(11, ow, wall.at[192:256]),
        local(12, norm, normv), local(13, mem, memv),
    ]
    loads += [local(14 + h, mixout.at[h], mixw.at[:, h]) for h in range(HEADS)]
    loads += [local(18, egate, egv), local(19, eup, euv), local(20, edown, edv)]
    loads[0].start()

    barrier = pltpu.get_barrier_semaphore()

    def along(d):
        return lax.rem(tp + 2 * d, NTP)

    def across(dy, dx):
        return lax.rem(ey + dy, 4) * 4 + lax.rem(ex + dx, 4)

    def greet(who):
        pl.semaphore_signal(barrier, inc=1, device_id=who, device_id_type=MESH)

    for d in FAR_Z:
        greet((ep, along(d)))
    for dy, dx in FAR_EP:
        greet((across(dy, dx), tp))
    greet((ep, other))
    for c in loads[1:]:
        c.start()

    i, j = iota((256, 256), 0), iota((256, 256), 1)
    perm[...] = (j == (((i >> 2) & 15) << 4) + ((i >> 6) << 2) + (i & 3)).astype(F32).astype(BF16)
    i, c = iota((256, 512), 0), iota((256, 512), 1)
    perm2[...] = (
        (((c >> 7) == ((i >> 2) & 3)) & ((c & 63) == ((i >> 4) << 2) + (i & 3))).astype(F32).astype(BF16)
    )

    def remote(src, dst, sent, got, who):
        return pltpu.make_async_remote_copy(
            src_ref=src, dst_ref=dst, send_sem=sent, recv_sem=got, device_id=who, device_id_type=MESH)

    def own_to(phase, buf, peer):
        return remote(buf.at[tp], buf.at[tp], ssem.at[phase, peer], rsem.at[phase, tp], (ep, peer))

    def forward(phase, buf, slot):
        return remote(buf.at[slot], buf.at[slot], fsem.at[phase, slot], rsem.at[phase, slot], (ep, other))

    def got(phase, buf, slot):
        remote(buf.at[slot], buf.at[slot], ssem.at[phase, slot], rsem.at[phase, slot], (ep, slot)).wait_recv()

    def gather_start(phase, buf):
        for d in FAR_Z:
            own_to(phase, buf, along(d)).start()
        own_to(phase, buf, other).start()

    def gather_pass(phase, buf):
        for d in (1, 7, 2, 6, 3, 5, 4):
            got(phase, buf, along(d))
            forward(phase, buf, along(d)).start()

    def gather_end(phase, buf):
        def step(d, _):
            got(phase, buf, lax.rem(other + 2 * d, NTP))
            return 0
        lax.fori_loop(0, 8, step, 0)

    def gather_sent(phase, buf):
        def step(d, _):
            own_to(phase, buf, along(d)).wait_send()
            forward(phase, buf, along(d)).wait_send()
            return 0
        lax.fori_loop(1, 8, step, 0)
        own_to(phase, buf, other).wait_send()

    def ep_copy(phase, src, dst, peer):
        return remote(src.at[peer], dst.at[ep], ssem.at[phase, peer], rsem.at[phase, ep], (peer, tp))

    def ep_start(phase, src, dst):
        for dy, dx in FAR_EP:
            ep_copy(phase, src, dst, across(dy, dx)).start()

    def ep_end(phase, dst):
        def step(d, _):
            peer = lax.rem(ep + d, NEP)
            remote(dst.at[peer], dst.at[peer], ssem.at[phase, peer], rsem.at[phase, peer], (peer, tp)).wait_recv()
            return 0
        lax.fori_loop(1, 16, step, 0)

    def ep_sent(phase, src, dst):
        def step(d, _):
            ep_copy(phase, src, dst, lax.rem(ep + d, NEP)).wait_send()
            return 0
        lax.fori_loop(1, 16, step, 0)

    pl.semaphore_wait(barrier, 23)
    loads[0].wait()
    gather_start(0, xg)

    for c in loads[1:8]:
        c.wait()
    sm[...] = jnp.zeros((128, 128), F32)
    sm[0:4, 0:64] = mss[...]
    sm[4:6, 0:64] = rws[...]
    sm[6:8, 0:64] = rts[...].astype(F32)
    cols = jnp.transpose(sm[...])[0:ROWS]
    w0, w1, r0, r1 = cols[:, 4:5], cols[:, 5:6], cols[:, 6:7], cols[:, 7:8]
    total = w0 + w1
    before = (iota((ROWS, ROWS), 1) < iota((ROWS, ROWS), 0)).astype(F32).astype(BF16)
    lane = iota((ROWS, 256), 1)
    slot_of = (lane & 3).astype(F32)
    expert = (lane >> 2).astype(F32)
    zero = jnp.zeros((ROWS, 256), F32)
    named0, named1 = r0 == expert, r1 == expert
    hit = jnp.where(named0 | named1, 1.0, zero)
    share = jnp.where(named0, w0 / total, zero) + jnp.where(named1, w1 / total, zero)
    share = jnp.where(nn(before, hit.astype(BF16)) == slot_of, share, zero)
    high = share.astype(BF16)
    comb[0:64] = high
    comb[64:128] = (share - high.astype(F32)).astype(BF16)
    expert = ((lane >> 4) * SPLIT + group).astype(F32)
    hit = jnp.where((r0 == expert) | (r1 == expert), 1.0, zero)
    pick = jnp.where(nn(before, hit.astype(BF16)) == slot_of, hit, zero)
    quarter = (lane >> 2) & 3
    for q in range(4):
        pbf[q * 64 : (q + 1) * 64] = jnp.where(quarter == q, pick, zero)
    pbt[...] = jnp.transpose(pbf[...]).astype(BF16)

    wgf[...] = jnp.zeros((16, WIDTH), F32)
    wgf[0:4] = igs[...].astype(F32)
    wgf[4:8] = fgs[...].astype(F32)
    wall[256:384] = jnp.zeros((128, WIDTH), BF16)
    wall[256:272] = wgf[...].astype(BF16)
    for c in loads[8:14]:
        c.wait()

    def narrow(k, _):
        at = pl.multiple_of(k * 8, 8)
        to = pl.multiple_of(k * 128, 128)
        for h in range(HEADS):
            memb[h, pl.ds(to, 128), :] = memv[pl.ds(at, 8), h].reshape(128, HDIM).astype(BF16)
        return 0

    lax.fori_loop(0, 8, narrow, 0)
    place = jnp.full((ROWS, 128), tp, jnp.int32)
    chosen = jnp.zeros((ROWS, 128), F32)
    for half in range(8):
        piece = normv[:, half // 2, (half % 2) * 128 : (half % 2 + 1) * 128]
        chosen = jnp.where(place >> 1 == half, piece, chosen)
    nso[...] = jnp.where((place & 1) == 1, pltpu.roll(chosen, 64, 1), chosen)

    gather_pass(0, xg)
    gather_end(0, xg)
    square = jnp.zeros((ROWS, 128), F32)
    for b in range(NTP):
        x = xg[b].astype(F32)
        square += x * x
        scaled[:, b * 128 : (b + 1) * 128] = (x * gms[b : b + 1, :]).astype(BF16)
    inverse = lax.rsqrt(jnp.sum(square, axis=1, keepdims=True) * (1.0 / WIDTH) + eps)
    acc = nt(scaled[...], wall[...]) * inverse
    lanes = iota((ROWS, 128), 1)
    low = lanes < 64
    low32 = low[0:32]
    qk = acc[:, 0:128] * jnp.where(low, 1.0, HDIM ** (-0.5))
    kq = pltpu.roll(qk, 64, 1)
    qb[tp] = jnp.where(low32, qk[0:32], kq[32:64]).astype(BF16)
    kb[tp] = jnp.where(low32, kq[0:32], qk[32:64]).astype(BF16)
    gather_start(1, qb)
    dot_n = jnp.sum(jnp.where(low, qk * nso[...], 0.0), axis=1, keepdims=True)
    dot_k = jnp.sum(jnp.where(low, qk * kq, 0.0), axis=1, keepdims=True)
    sm[0:64] = jnp.where(lanes == 0, dot_n, 0.0)
    sm[64:128] = jnp.where(lanes == 0, dot_k, 0.0)
    pb[tp] = jnp.transpose(sm[...])[0:1]
    gather_start(2, pb)

    vo = acc[:, 128:256]
    ov = pltpu.roll(vo, 64, 1)
    values = jnp.where(low, vo, ov)
    opened = jax.nn.sigmoid(jnp.where(low, ov, vo))
    ga = acc[:, 256:384]
    ingate = ga[:, 0:4]
    pre = pltpu.roll(ga, 124, 1)[:, 0:4] + bias[...]
    logforget = -(jnp.maximum(-pre, 0.0) + jnp.log1p(jnp.exp(-jnp.abs(pre))))
    carried = logforget + cols[:, 0:4]
    max_next = jnp.maximum(carried, ingate)
    decay = jnp.exp(carried - max_next)
    inflow = jnp.exp(ingate - max_next)
    floor = jnp.exp(-max_next)
    head = (lanes >> 4) & 3

    def spread(columns):
        out = jnp.broadcast_to(columns[0], (ROWS, 128))
        for h in range(1, HEADS):
            out = jnp.where(head == h, columns[h], out)
        return out

    def by_head(a):
        return [a[:, h : h + 1] for h in range(HEADS)]

    decay_l, inflow_l, floor_l = spread(by_head(decay)), spread(by_head(inflow)), spread(by_head(floor))
    pushed = inflow_l * values

    def settle(buf, out, k):
        c = pltpu.make_async_copy(buf, out, osem.at[k])
        c.start()
        return c

    outs = []
    sm[0:64] = pushed
    upt[...] = jnp.transpose(sm[...])[0:64]
    sm[0:64] = decay_l
    det[...] = jnp.transpose(sm[...])[0:64]
    sm[0:64, 0:4] = max_next
    mxt[...] = jnp.transpose(sm[...])[0:4, 0:64]
    outs += [settle(upt, update_out, 0), settle(det, decay_out, 1), settle(mxt, max_out, 2)]
    gather_sent(0, xg)

    def unpacked(buf, s):
        a, b = buf[2 * s].astype(F32), buf[2 * s + 1].astype(F32)
        top = jnp.where(low32, a, pltpu.roll(b, 64, 1))
        end = jnp.where(low32, pltpu.roll(a, 64, 1), b)
        return jnp.concatenate([top, end], axis=0)

    gather_pass(1, qb)
    gather_pass(2, pb)
    gather_end(1, qb)
    numerator = jnp.zeros((ROWS, 128), F32)
    mine = (lanes >> 4) == (iota((ROWS, 128), 0) & 7)
    for h in range(HEADS):
        q = jnp.concatenate([unpacked(qb, 2 * h), unpacked(qb, 2 * h + 1)], axis=1).astype(BF16)
        pieces = []
        for t in range(4):
            r = nt(q[t * 16 : (t + 1) * 16], memb[h, t * 256 : (t + 1) * 256])
            pieces += [r[0:8, 0:128], r[8:16, 128:256]]
        diagonal = jnp.where(mine, jnp.concatenate(pieces, axis=0), 0.0)
        for shift in (64, 32, 16):
            diagonal = diagonal + pltpu.roll(diagonal, shift, 1)
        numerator = jnp.where(head == h, diagonal, numerator)
    gather_end(2, pb)
    for h in range(HEADS):
        sm[h : h + 1] = (pb[4 * h] + pb[4 * h + 1]) + (pb[4 * h + 2] + pb[4 * h + 3])
    sums = jnp.transpose(sm[...])
    with_n = spread(by_head(sums[0:64]))
    with_k = spread(by_head(sums[64:128]))
    denominator = jnp.maximum(jnp.abs(decay_l * with_n + inflow_l * with_k), floor_l)
    gated = opened * ((decay_l * numerator + pushed * with_k) / denominator)
    gb[tp] = jnp.where(low32, gated[0:32], gated[32:64]).astype(BF16)
    gather_start(3, gb)
    gather_start(4, kb)

    for c in loads[14:]:
        c.wait()
    gather_sent(1, qb)
    gather_sent(2, pb)
    gather_pass(3, gb)
    gather_end(3, gb)
    heads = jnp.concatenate([unpacked(gb, s) for s in range(8)], axis=1).astype(BF16)
    square = jnp.zeros((ROWS, 128), F32)
    for n in range(4):
        part = nn(heads, mixw[:, :, :, n * 512 : (n + 1) * 512].reshape(1024, 512))
        for b in range(4):
            m = (xg[4 * n + b].astype(F32) + part[:, b * 128 : (b + 1) * 128]).astype(BF16)
            mid[4 * n + b] = m
            m = m.astype(F32)
            square += m * m
    inverse = lax.rsqrt(jnp.sum(square, axis=1, keepdims=True) * (1.0 / WIDTH) + eps)
    for b in range(NTP):
        nst[(b // 4) * 64 : (b // 4 + 1) * 64, (b % 4) * 128 : (b % 4 + 1) * 128] = (
            mid[b].astype(F32) * inverse * ges[b : b + 1, :]
        ).astype(BF16)
    sbuf[...] = nn(pbt[...], nst[...]).astype(BF16).reshape(NEP, 16, 512)
    ep_start(5, sbuf, rbuf)
    rbuf[ep] = sbuf[ep]

    gather_pass(4, kb)
    gather_sent(3, gb)
    gather_end(4, kb)
    for h in range(HEADS):
        k = jnp.concatenate([unpacked(kb, 2 * h), unpacked(kb, 2 * h + 1)], axis=1)
        keys[:, h, :] = k
        normv[:, h, :] = decay[:, h : h + 1] * normv[:, h, :] + inflow[:, h : h + 1] * k
    outs += [settle(keys, keys_out, 3), settle(normv, norm_out, 4)]

    ep_end(5, rbuf)
    rows = nn(perm[...], rbuf[...].reshape(256, 512)).astype(BF16)
    gate = jnp.zeros((ROWS, 256), F32)
    up = jnp.zeros((ROWS, 256), F32)
    for q in range(4):
        r = rows[q * 64 : (q + 1) * 64]
        gate += nn(r, egv[0, q * 512 : (q + 1) * 512, :])
        up += nn(r, euv[0, q * 512 : (q + 1) * 512, :])
    hidden = (gate * jax.nn.sigmoid(gate) * up).astype(BF16)
    for n in range(4):
        part = nn(hidden, edv[0, :, n * 512 : (n + 1) * 512])
        for b in range(4):
            piece = part[:, b * 128 : (b + 1) * 128]
            half32[b % 2, 2 * n + b // 2] = piece
            half16[b % 2, 2 * n + b // 2] = piece.astype(BF16)

    def to_other(z):
        return remote(half16.at[1 - core, z], pair.at[z], psem.at[0, z], psem.at[1, z], (ep, other))

    def to_owner(z):
        return remote(zsend.at[z], zbuf.at[chip], ssem.at[6, z], rsem.at[6, chip], (ep, 2 * z + core))

    def ahead(d):
        return lax.rem(chip + d, 8)

    for d in FAR_Z + (0,):
        to_other(ahead(d)).start()
    for d in FAR_Z:
        z = ahead(d)
        to_other(z).wait_recv()
        zsend[z] = (half32[core, z] + pair[z].astype(F32)).astype(BF16)
        to_owner(z).start()
    to_other(chip).wait_recv()
    zbuf[chip] = (half32[core, chip] + pair[chip].astype(F32)).astype(BF16)
    gather_sent(4, kb)
    ep_sent(5, sbuf, rbuf)

    def landed(d, _):
        z = ahead(d)
        remote(zbuf.at[z], zbuf.at[z], ssem.at[6, z], rsem.at[6, z], (ep, 2 * z + core)).wait_recv()
        return 0

    lax.fori_loop(1, 8, landed, 0)
    obuf[...] = nn(perm2[...], zbuf[...].reshape(512, 128)).astype(BF16).reshape(NEP, 16, 128)
    ep_start(7, obuf, fbuf)
    fbuf[ep] = obuf[ep]

    def left(d, _):
        to_other(ahead(d)).wait_send()
        return 0

    lax.fori_loop(0, 8, left, 0)

    def gone(d, _):
        to_owner(ahead(d)).wait_send()
        return 0

    lax.fori_loop(1, 8, gone, 0)
    for c in outs:
        c.wait()
    ep_end(7, fbuf)
    both = nn(comb[...], fbuf[...].reshape(256, 128))
    mixv[...] = (mid[tp].astype(F32) + (both[0:64] + both[64:128])).astype(BF16)
    last = settle(mixv, mixed, 5)
    ep_sent(7, obuf, fbuf)
    last.wait()


STEP = 8


def finish(mem, keys, update, decay, norm, maxt, mixed, memory_next, norm_next, max_next, mixed_next):
    at = lax.rem(128 - pl.program_id(0) * STEP, 128)
    u = pltpu.roll(update[...], at, 1)
    d = pltpu.roll(decay[...], at, 1)
    for b in range(STEP):
        for h in range(HEADS):
            uc = u[h * 16 : (h + 1) * 16, b : b + 1]
            dc = d[h * 16 : (h + 1) * 16, b : b + 1]
            memory_next[b, h] = dc * mem[b, h] + uc * keys[b, h : h + 1, :]
    norm_next[...] = norm[...]
    max_next[...] = maxt[...]
    mixed_next[...] = mixed[...]


def local(
    tokens, mixer_gain, expert_gain, query_weight, key_weight, value_weight, outgate_weight, ingate_weight,
    forget_weight, forget_bias, mixout_weight, memory_state, norm_state, max_state, expert_gate, expert_up,
    expert_down, routes, route_weights,
):
    hbm = pl.BlockSpec(memory_space=pl.ANY)
    vm = pl.BlockSpec(memory_space=pltpu.VMEM)
    v, dma = pltpu.VMEM, pltpu.SemaphoreType.DMA
    scratch = [
        v((NTP, ROWS, 128), BF16),
        v((384, WIDTH), BF16),
        v((4, WIDTH), BF16), v((4, WIDTH), BF16),
        v((16, WIDTH), F32),
        v((16, 128), F32), v((16, 128), F32),
        v((ROWS, HEADS, 16, HDIM), F32),
        v((HEADS, 1024, HDIM), BF16),
        v((ROWS, HEADS, HDIM), F32),
        v((NTP, HEADS, 16, WIDTH), BF16),
        v((1, WIDTH, 256), BF16), v((1, WIDTH, 256), BF16), v((1, 256, WIDTH), BF16),
        v((128, 128), F32),
        v((4, 64), F32), v((2, 64), jnp.int32), v((2, 64), F32),
        v((256, 256), BF16), v((256, 512), BF16),
        v((128, 256), BF16), v((256, 256), BF16), v((256, 256), F32),
        v((ROWS, 128), F32),
        v((ROWS, WIDTH), BF16),
        v((NTP, 32, 128), BF16), v((NTP, 32, 128), BF16), v((NTP, 1, 128), F32),
        v((NTP, 32, 128), BF16),
        v((NTP, ROWS, 128), BF16), v((256, 512), BF16),
        v((NEP, 16, 512), BF16), v((NEP, 16, 512), BF16),
        v((2, 8, ROWS, 128), F32), v((2, 8, ROWS, 128), BF16),
        v((8, ROWS, 128), BF16), v((8, ROWS, 128), BF16), v((8, ROWS, 128), BF16),
        v((NEP, 16, 128), BF16), v((NEP, 16, 128), BF16),
        v((ROWS, HEADS, HDIM), F32),
        v((64, 128), F32), v((64, 128), F32), v((HEADS, ROWS), F32), v((ROWS, 128), BF16),
        dma((21,)), dma((8, 16)), dma((5, 16)), dma((8, 16)), dma((2, 8)), dma((6,)),
    ]
    shape = jax.ShapeDtypeStruct
    mixed, keys, update, decay, norm_next, max_next = pl.pallas_call(
        body,
        out_shape=[
            shape((ROWS, 128), BF16), shape((ROWS, HEADS, HDIM), F32), shape((64, 128), F32), shape((64, 128), F32),
            shape((ROWS, HEADS, HDIM), F32), shape((HEADS, ROWS), F32),
        ],
        in_specs=[hbm] * 9 + [vm] + [hbm] * 9,
        out_specs=[hbm] * 6,
        scratch_shapes=scratch,
        compiler_params=pltpu.CompilerParams(
            collective_id=0, has_side_effects=True, vmem_limit_bytes=67043328
        ),
        name="step",
    )(
        tokens, mixer_gain.reshape(16, 128), expert_gain.reshape(16, 128),
        query_weight.T, key_weight.T,
        value_weight.transpose(1, 2, 0).reshape(64, WIDTH), outgate_weight.transpose(1, 2, 0).reshape(64, WIDTH),
        ingate_weight.T, forget_weight.T, forget_bias.reshape(1, HEADS),
        mixout_weight.reshape(HEADS, NTP, 16, WIDTH),
        memory_state, norm_state, max_state.T, expert_gate, expert_up, expert_down, routes.T, route_weights.T,
    )

    def rows(*rest):
        return pl.BlockSpec((STEP, *rest), lambda i: (i,) + (0,) * len(rest))

    def whole(*full):
        return pl.BlockSpec(full, lambda i: (0,) * len(full))

    memory_next, norm_next, max_next, mixed = pl.pallas_call(
        finish,
        grid=(ROWS // STEP,),
        out_shape=[
            shape(memory_state.shape, F32), shape((ROWS, HEADS, HDIM), F32), shape((HEADS, ROWS), F32),
            shape((ROWS, 128), BF16),
        ],
        in_specs=[
            rows(HEADS, 16, HDIM), rows(HEADS, HDIM), whole(64, 128), whole(64, 128), rows(HEADS, HDIM),
            whole(HEADS, ROWS), whole(ROWS, 128),
        ],
        out_specs=[rows(HEADS, 16, HDIM), rows(HEADS, HDIM), whole(HEADS, ROWS), whole(ROWS, 128)],
        compiler_params=pltpu.CompilerParams(vmem_limit_bytes=67043328),
        name="finish",
    )(memory_state, keys, update, decay, norm_next, max_next, mixed)
    return (mixed, memory_next, norm_next, max_next.T)


def solution(mesh):
    in_specs = (
        P("ep", "tp"), P(), P(), P(None, "tp"), P(None, "tp"), P(None, None, "tp"), P(None, None, "tp"), P(), P(), P(),
        P(), P("ep", None, "tp", None), P("ep", None, None), P("ep", None), P(("ep", "tp"), None, None),
        P(("ep", "tp"), None, None), P(("ep", "tp"), None, None), P("ep", None), P("ep", None),
    )
    out_specs = (P("ep", "tp"), P("ep", None, "tp", None), P("ep", None, None), P("ep", None))
    return jax.shard_map(local, mesh=mesh, in_specs=in_specs, out_specs=out_specs, check_vma=False)
```

time: 89.6 us -> 61.1 us (0.68)
  local copies, waits for them, and re-layouts: 20.7 us -> 0 us
  other arithmetic: 5.05 us -> 0 us
  Pallas kernels: 62.4 us -> 60.2 us
    unnamed x42 -> x0, local copies, waits for them, and re-layouts: 20.3 us -> none
    add x2 -> x0, other arithmetic: 5.04 us -> none  [the longest x1 4.13 us: local(): decay[:, :, None, None] * memory_state]
    pallas_call x1 -> x2, Pallas kernels: 62.4 us -> 60.2 us  [the longest x1 52.5 us: local(): pl.pallas_call(body, out_shape=[shape((ROWS, 128), BF16), shape((ROWS, HE...]
where the time goes in v2:
time: 61.1 us; the launch traced here: 60.9 us
  Pallas kernels  60.2 us (99%)
  between operations  0.65 us (1%)
    pallas_call x1, Pallas kernels, local(): pl.pallas_call(body, out_shape=[shape((ROWS, 128), BF16), shape((ROWS, HE...  52.5 us
    pallas_call x1, Pallas kernels, local(): pl.pallas_call(finish, grid=(ROWS // STEP,), out_shape=[shape(memory_stat...  7.69 us

profile of v2, /device:TPU:1, one launch (start us, length us, event | category | flops | bytes accessed | tf_op | source)
XLA Modules:
  0.0 60.9 jit_solution(1189578589200469377)
XLA Ops:
  0.6 52.5 %step.1 = (bf16[64,128]{1,0:T(8,128)(2,1)}, f32[64,4,256]{2,1,0:T(4,128)}, f32[64,128]{1,0:T(8,128)}, f32[64,128]{1,0:T(8,128)}, f32[64,4,256]{2,1,0:T(4,128)}, /*index=5*/f32[4,64]{1,0:T(4,128)}) custom-call(bf16[64,128]{1,0:T(8,128)(2,1)} %tok.1, f32[16,128]{1,0:T(8,128)} %bitcast.25, f32[16,128]{1,0:T(8,128)} %bitcast.26, bf16[64,2048]{1,0:T(8,128)(2,1)} %bitcast.19, ...), custom_call_target="tpu_custom_call" | custom-call | tf_op jit(solution)/shard_map/step/pallas_call | solution.py:451
  53.2 7.7 %finish.1 = (f32[64,4,16,256]{3,2,1,0:T(8,128)}, f32[64,4,256]{2,1,0:T(4,128)}, f32[4,64]{1,0:T(4,128)}, bf16[64,128]{1,0:T(8,128)(2,1)}) custom-call(f32[64,4,16,256]{3,2,1,0:T(8,128)} %mem.3, f32[64,4,256]{2,1,0:T(4,128)} %get-tuple-element.14.keys, f32[64,128]{1,0:T(8,128)} %get-tuple-element.15.update, f32[64,128]{1,0:T(8,128)} %get-tuple-element.16.decay, ...), custom_call_target="tpu_custom_call" | custom-call | tf_op jit(solution)/shard_map/finish/pallas_call | solution.py:479

commit v3 on v2

--- a/solution.py
+++ b/solution.py
@@ -25,19 +25,24 @@
 
 FAR_EP = sorted(((dy, dx) for dy in range(4) for dx in range(4) if dy or dx), key=lambda p: (-(min(p[0], 4 - p[0]) + min(p[1], 4 - p[1])), p))
 FAR_Z = (4, 3, 5, 2, 6, 1, 7)
+DIRECT = (1, 2, 3)
+
+
+STEP = 8
 
 
 def body(
     tok, gain_m, gain_e, qw, kw, vw, ow, igw, fgw, bias, mixout, mem, norm, mstate, egate, eup, edown, rt, rw,
-    mixed, keys_out, update_out, decay_out, norm_out, max_out,
+    mixed, mem_out, norm_out, max_out,
     xg, wall, igs, fgs, wgf, gms, ges, memv, memb, normv, mixw, egv, euv, edv, sm, mss, rts, rws, perm, perm2,
-    comb, pbt, pbf, nso, scaled, qb, kb, pb, gb, mid, nst, sbuf, rbuf, half32, half16, pair, zsend, zbuf, obuf, fbuf,
+    comb, pbt, pbf, nso, biasv, scaled, qb, kb, pb, gb, mid, nst, sbuf, rbuf, half32, half16, pair, zsend, zbuf, obuf, fbuf,
     keys, upt, det, mxt, mixv,
     lsem, ssem, fsem, rsem, psem, osem,
 ):
     ep, tp = lax.axis_index("ep"), lax.axis_index("tp")
     group, chip, core = tp // SPLIT, tp // 2, tp % 2
     other = chip * 2 + (1 - core)
+    opposite = lax.rem(other + 8, NTP)
     ey, ex = ep // 4, ep % 4
 
     def local(i, src, dst):
@@ -52,6 +57,7 @@
         local(12, norm, normv), local(13, mem, memv),
     ]
     loads += [local(14 + h, mixout.at[h], mixw.at[:, h]) for h in range(HEADS)]
+    loads += [local(21, bias, biasv)]
     loads += [local(18, egate, egv), local(19, eup, euv), local(20, edown, edv)]
     loads[0].start()
 
@@ -71,6 +77,7 @@
     for dy, dx in FAR_EP:
         greet((across(dy, dx), tp))
     greet((ep, other))
+    greet((ep, opposite))
     for c in loads[1:]:
         c.start()
 
@@ -97,10 +104,12 @@
     def gather_start(phase, buf):
         for d in FAR_Z:
             own_to(phase, buf, along(d)).start()
+            if d == 4 and phase in DIRECT:
+                own_to(phase, buf, opposite).start()
         own_to(phase, buf, other).start()
 
     def gather_pass(phase, buf):
-        for d in (1, 7, 2, 6, 3, 5, 4):
+        for d in (1, 7, 2, 6, 3, 5) if phase in DIRECT else (1, 7, 2, 6, 3, 5, 4):
             got(phase, buf, along(d))
             forward(phase, buf, along(d)).start()
 
@@ -109,14 +118,19 @@
             got(phase, buf, lax.rem(other + 2 * d, NTP))
             return 0
         lax.fori_loop(0, 8, step, 0)
+        if phase in DIRECT:
+            got(phase, buf, along(4))
 
     def gather_sent(phase, buf):
         def step(d, _):
             own_to(phase, buf, along(d)).wait_send()
-            forward(phase, buf, along(d)).wait_send()
             return 0
         lax.fori_loop(1, 8, step, 0)
         own_to(phase, buf, other).wait_send()
+        if phase in DIRECT:
+            own_to(phase, buf, opposite).wait_send()
+        for d in (1, 7, 2, 6, 3, 5) if phase in DIRECT else (1, 7, 2, 6, 3, 5, 4):
+            forward(phase, buf, along(d)).wait_send()
 
     def ep_copy(phase, src, dst, peer):
         return remote(src.at[peer], dst.at[ep], ssem.at[phase, peer], rsem.at[phase, ep], (peer, tp))
@@ -138,11 +152,11 @@
             return 0
         lax.fori_loop(1, 16, step, 0)
 
-    pl.semaphore_wait(barrier, 23)
+    pl.semaphore_wait(barrier, 24)
     loads[0].wait()
     gather_start(0, xg)
 
-    for c in loads[1:8]:
+    for c in loads[1:8] + loads[18:19]:
         c.wait()
     sm[...] = jnp.zeros((128, 128), F32)
     sm[0:4, 0:64] = mss[...]
@@ -224,7 +238,7 @@
     opened = jax.nn.sigmoid(jnp.where(low, ov, vo))
     ga = acc[:, 256:384]
     ingate = ga[:, 0:4]
-    pre = pltpu.roll(ga, 124, 1)[:, 0:4] + bias[...]
+    pre = pltpu.roll(ga, 124, 1)[:, 0:4] + biasv[...]
     logforget = -(jnp.maximum(-pre, 0.0) + jnp.log1p(jnp.exp(-jnp.abs(pre))))
     carried = logforget + cols[:, 0:4]
     max_next = jnp.maximum(carried, ingate)
@@ -257,7 +271,7 @@
     det[...] = jnp.transpose(sm[...])[0:64]
     sm[0:64, 0:4] = max_next
     mxt[...] = jnp.transpose(sm[...])[0:4, 0:64]
-    outs += [settle(upt, update_out, 0), settle(det, decay_out, 1), settle(mxt, max_out, 2)]
+    outs += [settle(mxt, max_out, 0)]
     gather_sent(0, xg)
 
     def unpacked(buf, s):
@@ -268,6 +282,7 @@
 
     gather_pass(1, qb)
     gather_pass(2, pb)
+    gather_start(4, kb)
     gather_end(1, qb)
     numerator = jnp.zeros((ROWS, 128), F32)
     mine = (lanes >> 4) == (iota((ROWS, 128), 0) & 7)
@@ -291,13 +306,13 @@
     gated = opened * ((decay_l * numerator + pushed * with_k) / denominator)
     gb[tp] = jnp.where(low32, gated[0:32], gated[32:64]).astype(BF16)
     gather_start(3, gb)
-    gather_start(4, kb)
-
-    for c in loads[14:]:
+
+    for c in loads[14:18] + loads[19:]:
         c.wait()
     gather_sent(1, qb)
     gather_sent(2, pb)
     gather_pass(3, gb)
+    gather_pass(4, kb)
     gather_end(3, gb)
     heads = jnp.concatenate([unpacked(gb, s) for s in range(8)], axis=1).astype(BF16)
     square = jnp.zeros((ROWS, 128), F32)
@@ -317,14 +332,31 @@
     ep_start(5, sbuf, rbuf)
     rbuf[ep] = sbuf[ep]
 
-    gather_pass(4, kb)
     gather_sent(3, gb)
     gather_end(4, kb)
     for h in range(HEADS):
         k = jnp.concatenate([unpacked(kb, 2 * h), unpacked(kb, 2 * h + 1)], axis=1)
         keys[:, h, :] = k
         normv[:, h, :] = decay[:, h : h + 1] * normv[:, h, :] + inflow[:, h : h + 1] * k
-    outs += [settle(keys, keys_out, 3), settle(normv, norm_out, 4)]
+    outs += [settle(normv, norm_out, 1)]
+
+    def stored(k):
+        at = pl.multiple_of(k * STEP, STEP)
+        return pltpu.make_async_copy(memv.at[pl.ds(at, STEP)], mem_out.at[pl.ds(at, STEP)], osem.at[5 + k])
+
+    def renew(k, _):
+        shift = lax.rem(128 - k * STEP, 128)
+        u = pltpu.roll(upt[...], shift, 1)
+        d = pltpu.roll(det[...], shift, 1)
+        for b in range(STEP):
+            for h in range(HEADS):
+                uc = u[h * 16 : (h + 1) * 16, b : b + 1]
+                dc = d[h * 16 : (h + 1) * 16, b : b + 1]
+                memv[k * STEP + b, h] = dc * memv[k * STEP + b, h] + uc * keys[k * STEP + b, h : h + 1, :]
+        stored(k).start()
+        return 0
+
+    lax.fori_loop(0, 3, renew, 0)
 
     ep_end(5, rbuf)
     rows = nn(perm[...], rbuf[...].reshape(256, 512)).astype(BF16)
@@ -360,6 +392,7 @@
         to_owner(z).start()
     to_other(chip).wait_recv()
     zbuf[chip] = (half32[core, chip] + pair[chip].astype(F32)).astype(BF16)
+    lax.fori_loop(3, 6, renew, 0)
     gather_sent(4, kb)
     ep_sent(5, sbuf, rbuf)
 
@@ -373,6 +406,8 @@
     ep_start(7, obuf, fbuf)
     fbuf[ep] = obuf[ep]
 
+    lax.fori_loop(6, 8, renew, 0)
+
     def left(d, _):
         to_other(ahead(d)).wait_send()
         return 0
@@ -386,29 +421,32 @@
     lax.fori_loop(1, 8, gone, 0)
     for c in outs:
         c.wait()
+
+    def kept(k, _):
+        stored(k).wait()
+        return 0
+
+    lax.fori_loop(0, 8, kept, 0)
     ep_end(7, fbuf)
     both = nn(comb[...], fbuf[...].reshape(256, 128))
     mixv[...] = (mid[tp].astype(F32) + (both[0:64] + both[64:128])).astype(BF16)
-    last = settle(mixv, mixed, 5)
+    last = settle(mixv, mixed, 2)
     ep_sent(7, obuf, fbuf)
     last.wait()
 
 
-STEP = 8
-
-
-def finish(mem, keys, update, decay, norm, maxt, mixed, memory_next, norm_next, max_next, mixed_next):
-    at = lax.rem(128 - pl.program_id(0) * STEP, 128)
-    u = pltpu.roll(update[...], at, 1)
-    d = pltpu.roll(decay[...], at, 1)
-    for b in range(STEP):
-        for h in range(HEADS):
-            uc = u[h * 16 : (h + 1) * 16, b : b + 1]
-            dc = d[h * 16 : (h + 1) * 16, b : b + 1]
-            memory_next[b, h] = dc * mem[b, h] + uc * keys[b, h : h + 1, :]
-    norm_next[...] = norm[...]
-    max_next[...] = maxt[...]
-    mixed_next[...] = mixed[...]
+def finish(mem, norm, maxt, mixed, mem_to, norm_to, max_to, mixed_to, held, normv, maxv, mixv, came, went):
+    pairs = [(mem.at[pl.ds(k * STEP, STEP)], held.at[pl.ds(k * STEP, STEP)], mem_to.at[pl.ds(k * STEP, STEP)]) for k in range(8)]
+    pairs += [(norm, normv, norm_to), (maxt, maxv, max_to), (mixed, mixv, mixed_to)]
+    ins = [pltpu.make_async_copy(a, b, came.at[k]) for k, (a, b, _) in enumerate(pairs)]
+    outs = [pltpu.make_async_copy(b, c, went.at[k]) for k, (_, b, c) in enumerate(pairs)]
+    for c in ins:
+        c.start()
+    for c, o in zip(ins, outs):
+        c.wait()
+        o.start()
+    for o in outs:
+        o.wait()
 
 
 def local(
@@ -417,7 +455,6 @@
     expert_down, routes, route_weights,
 ):
     hbm = pl.BlockSpec(memory_space=pl.ANY)
-    vm = pl.BlockSpec(memory_space=pltpu.VMEM)
     v, dma = pltpu.VMEM, pltpu.SemaphoreType.DMA
     scratch = [
         v((NTP, ROWS, 128), BF16),
@@ -434,7 +471,7 @@
         v((4, 64), F32), v((2, 64), jnp.int32), v((2, 64), F32),
         v((256, 256), BF16), v((256, 512), BF16),
         v((128, 256), BF16), v((256, 256), BF16), v((256, 256), F32),
-        v((ROWS, 128), F32),
+        v((ROWS, 128), F32), v((1, HEADS), F32),
         v((ROWS, WIDTH), BF16),
         v((NTP, 32, 128), BF16), v((NTP, 32, 128), BF16), v((NTP, 1, 128), F32),
         v((NTP, 32, 128), BF16),
@@ -445,17 +482,17 @@
         v((NEP, 16, 128), BF16), v((NEP, 16, 128), BF16),
         v((ROWS, HEADS, HDIM), F32),
         v((64, 128), F32), v((64, 128), F32), v((HEADS, ROWS), F32), v((ROWS, 128), BF16),
-        dma((21,)), dma((8, 16)), dma((5, 16)), dma((8, 16)), dma((2, 8)), dma((6,)),
+        dma((22,)), dma((8, 16)), dma((5, 16)), dma((8, 16)), dma((2, 8)), dma((13,)),
     ]
     shape = jax.ShapeDtypeStruct
-    mixed, keys, update, decay, norm_next, max_next = pl.pallas_call(
+    mixed, memory_next, norm_next, max_next = pl.pallas_call(
         body,
         out_shape=[
-            shape((ROWS, 128), BF16), shape((ROWS, HEADS, HDIM), F32), shape((64, 128), F32), shape((64, 128), F32),
-            shape((ROWS, HEADS, HDIM), F32), shape((HEADS, ROWS), F32),
+            shape((ROWS, 128), BF16), shape(memory_state.shape, F32), shape((ROWS, HEADS, HDIM), F32),
+            shape((HEADS, ROWS), F32),
         ],
-        in_specs=[hbm] * 9 + [vm] + [hbm] * 9,
-        out_specs=[hbm] * 6,
+        in_specs=[hbm] * 19,
+        out_specs=[hbm] * 4,
         scratch_shapes=scratch,
         compiler_params=pltpu.CompilerParams(
             collective_id=0, has_side_effects=True, vmem_limit_bytes=67043328
@@ -470,27 +507,16 @@
         memory_state, norm_state, max_state.T, expert_gate, expert_up, expert_down, routes.T, route_weights.T,
     )
 
-    def rows(*rest):
-        return pl.BlockSpec((STEP, *rest), lambda i: (i,) + (0,) * len(rest))
-
-    def whole(*full):
-        return pl.BlockSpec(full, lambda i: (0,) * len(full))
-
+    kinds = [((ROWS, HEADS, 16, HDIM), F32), ((ROWS, HEADS, HDIM), F32), ((HEADS, ROWS), F32), ((ROWS, 128), BF16)]
     memory_next, norm_next, max_next, mixed = pl.pallas_call(
         finish,
-        grid=(ROWS // STEP,),
-        out_shape=[
-            shape(memory_state.shape, F32), shape((ROWS, HEADS, HDIM), F32), shape((HEADS, ROWS), F32),
-            shape((ROWS, 128), BF16),
-        ],
-        in_specs=[
-            rows(HEADS, 16, HDIM), rows(HEADS, HDIM), whole(64, 128), whole(64, 128), rows(HEADS, HDIM),
-            whole(HEADS, ROWS), whole(ROWS, 128),
-        ],
-        out_specs=[rows(HEADS, 16, HDIM), rows(HEADS, HDIM), whole(HEADS, ROWS), whole(ROWS, 128)],
+        out_shape=[shape(*k) for k in kinds],
+        in_specs=[hbm] * 4,
+        out_specs=[hbm] * 4,
+        scratch_shapes=[v(*k) for k in kinds] + [dma((11,)), dma((11,))],
         compiler_params=pltpu.CompilerParams(vmem_limit_bytes=67043328),
         name="finish",
-    )(memory_state, keys, update, decay, norm_next, max_next, mixed)
+    )(memory_next, norm_next, max_next, mixed)
     return (mixed, memory_next, norm_next, max_next.T)
 
 

time: 61.1 us -> 57 us (0.933)
  Pallas kernels: 60.2 us -> 56.3 us
    pallas_call x2, Pallas kernels: 60.2 us -> 56.3 us  [the longest x1 52.4 us: local(): pl.pallas_call(body, out_shape=[shape((ROWS, 128), BF16), shape(memory_st...]
where the time goes in v3:
time: 57 us; the launch traced here: 56.9 us
  Pallas kernels  56.3 us (99%)
  between operations  0.65 us (1%)
    pallas_call x1, Pallas kernels, local(): pl.pallas_call(body, out_shape=[shape((ROWS, 128), BF16), shape(memory_st...  52.4 us
    pallas_call x1, Pallas kernels, local(): pl.pallas_call(finish, out_shape=[shape(*k) for k in kinds], in_specs=[hb...  3.82 us

profile of v3, /device:TPU:1, one launch (start us, length us, event | category | flops | bytes accessed | tf_op | source)
XLA Modules:
  0.0 56.9 jit_solution(9613224761627244523)
XLA Ops:
  0.6 52.4 %step.1 = (bf16[64,128]{1,0:T(8,128)(2,1)}, f32[64,4,16,256]{3,2,1,0:T(8,128)}, f32[64,4,256]{2,1,0:T(4,128)}, f32[4,64]{1,0:T(4,128)}) custom-call(bf16[64,128]{1,0:T(8,128)(2,1)} %tok.1, f32[16,128]{1,0:T(8,128)} %bitcast.25, f32[16,128]{1,0:T(8,128)} %bitcast.26, bf16[64,2048]{1,0:T(8,128)(2,1)} %bitcast.19, bf16[64,2048]{1,0:T(8,128)(2,1)} %bitcast.20, ...), custom_call_target="tpu_custom_call" | custom-call | tf_op jit(solution)/shard_map/step/pallas_call | solution.py:488
  53.1 3.8 %finish.1 = (f32[64,4,16,256]{3,2,1,0:T(8,128)}, f32[64,4,256]{2,1,0:T(4,128)}, f32[4,64]{1,0:T(4,128)}, bf16[64,128]{1,0:T(8,128)(2,1)}) custom-call(f32[64,4,16,256]{3,2,1,0:T(8,128)} %get-tuple-element.12.mem, f32[64,4,256]{2,1,0:T(4,128)} %get-tuple-element.13.norm, f32[4,64]{1,0:T(4,128)} %get-tuple-element.14.maxt, bf16[64,128]{1,0:T(8,128)(2,1)} %get-tuple-element.15.mixed), custom_call_target="tpu_custom_call" | custom-call | tf_op jit(solution)/shard_map/finish/pallas_call | solution.py:511
